TPU v7x, 32 devices: a whole 2x2x4 slice. The times are simulated.
32 devices in a mesh: sp: 8 (over z, x), tp: 4 (over y, core).
Axes of the slice: x: 2, y: 2, z: 4, core: 2. Of those that a mesh axis runs over, the one named last changes fastest.
Arguments:
- query_a: bfloat16 [1024, 2048], P('sp', 'tp'), may hold values from -6 to 6
- key_a: bfloat16 [1024, 2048], P('sp', 'tp'), may hold values from -6 to 6
- value_a: bfloat16 [1024, 4096], P('sp', 'tp'), may hold values from -6 to 6
- query_b: bfloat16 [1024, 2048], P('sp', 'tp'), may hold values from -6 to 6
- key_b: bfloat16 [1024, 2048], P('sp', 'tp'), may hold values from -6 to 6
- value_b: bfloat16 [1024, 2048], P('sp', 'tp'), may hold values from -6 to 6
- in_gate: float32 [2, 2, 16, 1024], P(None, None, 'tp', 'sp'), may hold values from -6 to 300
- forget_gate: float32 [2, 2, 16, 1024], P(None, None, 'tp', 'sp'), may hold values from 0 to 14.1
- head_gain_a: float32 [16, 256], P('tp'), may hold values from 0.1 to 1.9
- head_gain_b: float32 [16, 128], P('tp'), may hold values from 0.1 to 1.9
- out_weight_a: bfloat16 [4096, 2048], P('tp'), may hold values from -0.078125 to 0.078125
- out_weight_b: bfloat16 [2048, 2048], P('tp'), may hold values from -0.078125 to 0.078125
- residual: bfloat16 [2048, 1024], P('tp', 'sp'), may hold values from -40 to 40
- norm_gain: float32 [2048], P('tp'), may hold values from 0.1 to 1.9
- routes: int32 [1024, 2], P('sp'), may hold values from 0 to 7, all different within a row; in each aligned block of 128 rows (0 to 127, 128 to 255, ...) at most 64 rows name the same one
- route_weights: float32 [1024, 2], P('sp'), may hold values from 0.2 to 1
- expert_gate: bfloat16 [8, 2048, 4096], P('sp', None, 'tp'), may hold values from -0.125 to 0.125
- expert_up: bfloat16 [8, 2048, 4096], P('sp', None, 'tp'), may hold values from -0.125 to 0.125
- expert_down: bfloat16 [8, 4096, 2048], P('sp', 'tp'), may hold values from -0.09375 to 0.09375
Outputs:
- layer_output: bfloat16 [2048, 1024], P('tp', 'sp')
Inputs may be any that keep to these rules, and one draw needn't show every extreme that they name: `routes`: each row names 2 different experts. In each aligned block of 128 rows (the rows of one index of sp) no expert is named by more than 64 rows, a bound that some blocks reach.
All inputs are finite; a program needn't handle non-finite values.
Results may differ from a plain program's by a relative error of at most 0.012.
Values may be sent and summed in bfloat16 or wider, within the bound.
A program may use at most 128 MiB of HBM per device.

v0:
```python
import functools

import jax
import jax.numpy as jnp
from jax import lax
from jax.experimental import pallas as pl
from jax.experimental.pallas import tpu as pltpu
from jax.sharding import PartitionSpec as P

EPSILON = 1e-06
NOTHING = -1e30


def dot(left, right, contract):
    return lax.dot_general(
        left, right, (contract, ((), ())), preferred_element_type=jnp.float32
    )


MESH = pl.DeviceIdType.MESH


def greet(peers):
    barrier = pltpu.get_barrier_semaphore()
    for peer in peers:
        pl.semaphore_signal(barrier, inc=1, device_id=peer, device_id_type=MESH)
    pl.semaphore_wait(barrier, len(peers))


def exchange_kernel(count, arrays, *refs):
    given, taken = refs[:arrays], refs[arrays : 2 * arrays]
    sent, landed, kept = refs[2 * arrays :]
    mine = lax.axis_index("sp")
    peers = [lax.rem(mine + step, count) for step in range(1, count)]
    greet([{"sp": peer} for peer in peers])
    copies = []
    for step, peer in enumerate(peers):
        for a in range(arrays):
            copy = pltpu.make_async_remote_copy(
                src_ref=given[a].at[peer],
                dst_ref=taken[a].at[mine],
                send_sem=sent.at[a, step],
                recv_sem=landed.at[a, step],
                device_id={"sp": peer},
                device_id_type=MESH,
            )
            copy.start()
            copies.append(copy)
    for a in range(arrays):
        copy = pltpu.make_async_copy(given[a].at[mine], taken[a].at[mine], kept.at[a])
        copy.start()
        copies.append(copy)
    for copy in copies:
        copy.wait()


def exchange(arrays, number):
    count = arrays[0].shape[0]
    spec = pl.BlockSpec(memory_space=pltpu.VMEM)
    return pl.pallas_call(
        functools.partial(exchange_kernel, count, len(arrays)),
        out_shape=[jax.ShapeDtypeStruct(a.shape, a.dtype) for a in arrays],
        in_specs=[spec] * len(arrays),
        out_specs=[spec] * len(arrays),
        scratch_shapes=[
            pltpu.SemaphoreType.DMA((len(arrays), count - 1)),
            pltpu.SemaphoreType.DMA((len(arrays), count - 1)),
            pltpu.SemaphoreType.DMA((len(arrays),)),
        ],
        compiler_params=pltpu.CompilerParams(collective_id=number, has_side_effects=True),
    )(*arrays)


def dispatch_kernel(count, across, given, taken, sent, landed, kept, y_sent, y_landed, c_sent, c_landed):
    mine, slot = lax.axis_index("sp"), lax.axis_index("tp")
    chips = across // 2
    width = given.shape[-1]
    twin = slot + 1 - 2 * lax.rem(slot, 2)
    others = [lax.rem(slot + 2 * step, across) for step in range(1, chips)]
    behind = [lax.rem(slot + across - 2 * step, across) for step in range(1, chips)]
    peers = [lax.rem(mine + step, count) for step in range(1, count)]
    greet([{"sp": peer} for peer in peers] + [{"tp": other} for other in others] + [{"tp": twin}])

    def place(source, owner):
        return taken.at[source, :, pl.ds(pl.multiple_of(owner * width, width), width)]

    def forward(source, owner, target, send, land):
        copy = pltpu.make_async_remote_copy(
            src_ref=place(source, owner),
            dst_ref=place(source, owner),
            send_sem=send,
            recv_sem=land,
            device_id={"tp": target},
            device_id_type=MESH,
        )
        copy.start()
        return copy

    own = pltpu.make_async_copy(given.at[mine], place(mine, slot), kept.at[0])
    own.start()
    first = []
    for step, peer in enumerate(peers):
        copy = pltpu.make_async_remote_copy(
            src_ref=given.at[peer],
            dst_ref=place(mine, slot),
            send_sem=sent.at[step],
            recv_sem=landed.at[step],
            device_id={"sp": peer},
            device_id_type=MESH,
        )
        copy.start()
        first.append(copy)
    sources = [lax.rem(mine + count - step, count) for step in range(count)]
    along, last = [], []

    def hand_over(step):
        for turn, owner in enumerate(behind):
            along[step][turn].wait_recv()
            last.append(
                forward(
                    sources[step], owner, twin, c_sent.at[step, turn + 1], c_landed.at[step, turn + 1]
                )
            )

    for step in range(count):
        if step == 0:
            own.wait()
        else:
            first[step - 1].wait_recv()
        along.append(
            [
                forward(sources[step], slot, other, y_sent.at[step, turn], y_landed.at[step, turn])
                for turn, other in enumerate(others)
            ]
        )
        last.append(forward(sources[step], slot, twin, c_sent.at[step, 0], c_landed.at[step, 0]))
        if step > 0:
            hand_over(step - 1)
    hand_over(count - 1)
    for copy in first:
        copy.wait_send()
    for copies in along:
        for copy in copies:
            copy.wait_send()
    for copy in last:
        copy.wait()


def dispatch_rows(buffer, number):
    count, rows, width = buffer.shape
    across = lax.axis_size("tp")
    chips = across // 2
    spec = pl.BlockSpec(memory_space=pltpu.VMEM)
    dma = pltpu.SemaphoreType.DMA
    return pl.pallas_call(
        functools.partial(dispatch_kernel, count, across),
        out_shape=jax.ShapeDtypeStruct((count, rows, width * across), buffer.dtype),
        in_specs=[spec],
        out_specs=spec,
        scratch_shapes=[
            dma((count - 1,)), dma((count - 1,)), dma((1,)),
            dma((count, chips - 1)), dma((count, chips - 1)),
            dma((count, chips)), dma((count, chips)),
        ],
        compiler_params=pltpu.CompilerParams(collective_id=number, has_side_effects=True),
    )(buffer)


def one_head(query, key, value, keys, values, inner_row, outer_row, column, peak, gain, share):
    length, width_k = query.shape
    scale = width_k ** (-0.5)
    rows = lax.broadcasted_iota(jnp.int32, (length, length), 0)
    lanes = lax.broadcasted_iota(jnp.int32, (length, length), 1)
    near = dot(query, key, ((1,), (1,))) * scale
    far = dot(query, keys, ((1,), (1,))) * scale
    far_scores = [far * outer_row[r] for r in range(2)]
    far_sums = [jnp.sum(scores, axis=1, keepdims=True) for scores in far_scores]
    far_values = dot(
        jnp.concatenate([scores.astype(jnp.bfloat16) for scores in far_scores], axis=0),
        values,
        ((1,), (0,)),
    )
    both = None
    for r in range(2):
        keep = lanes <= rows if r == 0 else lanes >= rows
        logs = jnp.where(keep, column[r] + inner_row[r], NOTHING)
        carried_log = column[r] + peak[r]
        top = jnp.maximum(carried_log, jnp.max(logs, axis=1, keepdims=True))
        carried = jnp.exp(carried_log - top)
        scores = near * jnp.exp(logs - top)
        numer = carried * far_values[r * length : (r + 1) * length] + dot(
            scores.astype(jnp.bfloat16), value, ((1,), (0,))
        )
        denom = carried * far_sums[r] + jnp.sum(scores, axis=1, keepdims=True)
        out = numer / jnp.maximum(jnp.abs(denom), jnp.exp(-top))
        both = out if both is None else both + out
    mean = jnp.sum(both * both, axis=1, keepdims=True) * share
    return (both * lax.rsqrt(mean + EPSILON) * gain).astype(jnp.bfloat16)


def mixer_kernel(
    qa, ka, va, qb, kb, vb, all_ka, all_va, all_kb, all_vb,
    inner, outer, column, peak, gain_a, gain_b, heads_a, heads_b,
):
    parts = (
        (qa, ka, va, all_ka, all_va, gain_a, heads_a),
        (qb, kb, vb, all_kb, all_vb, gain_b, heads_b),
    )
    for g, (q, k, v, every_k, every_v, gain, heads) in enumerate(parts):
        heads[...] = one_head(
            q[...], k[...], v[...], every_k[...], every_v[...],
            [inner[0, 2 * r + g : 2 * r + g + 1, :] for r in range(2)],
            [outer[0, 2 * r + g : 2 * r + g + 1, :] for r in range(2)],
            [column[0, :, 2 * r + g : 2 * r + g + 1] for r in range(2)],
            [peak[0, 2 * r + g : 2 * r + g + 1, 0:1] for r in range(2)],
            gain[0],
            1.0 / gain.shape[-1],
        )


def mix_heads(query_a, key_a, value_a, query_b, key_b, value_b, in_gate, forget_gate, gain_a, gain_b):
    heads = gain_a.shape[0]
    length = query_a.shape[0]
    width_k = query_a.shape[1] // heads
    width_a, width_b = gain_a.shape[1], gain_b.shape[1]
    count, mine = lax.axis_size("sp"), lax.axis_index("sp")
    packed = jnp.concatenate([value_a, key_a, key_b, value_b], axis=1)
    gathered = lax.all_gather(packed, "sp", axis=0, tiled=True)
    total_rows = gathered.shape[0]
    log_decay = jax.nn.log_sigmoid(forget_gate)
    ones = jnp.ones((length, length), jnp.float32)
    exact = lax.Precision.HIGHEST
    run = jnp.stack(
        [
            jnp.einsum("ghs,st->ght", log_decay[0], jnp.triu(ones), precision=exact),
            jnp.einsum("ghs,st->ght", log_decay[1], jnp.tril(ones), precision=exact),
        ]
    )
    whole = jnp.sum(log_decay, axis=-1, keepdims=True)
    tails = in_gate + whole - run
    small = lax.all_gather(
        jnp.stack([tails, jnp.broadcast_to(whole, tails.shape)]), "sp", axis=0
    )
    every_tail, every_whole = small[:, 0], small[:, 1, ..., 0]
    place = jnp.arange(count)
    source, middle = place[:, None], place[None, :]
    between = jnp.stack(
        [
            (middle > source) & (middle < mine),
            (middle < source) & (middle > mine),
        ]
    ).astype(jnp.float32)
    gap = jnp.sum(between[:, :, :, None, None] * jnp.moveaxis(every_whole, 0, 1)[:, None], axis=2)
    seen = jnp.stack([place < mine, place > mine])[:, :, None, None, None]
    logs = jnp.where(seen, jnp.moveaxis(every_tail, 0, 1) + gap[..., None], NOTHING)
    peak = jnp.max(logs, axis=(1, 4))
    outer = jnp.where(seen, jnp.exp(logs - peak[:, None, :, :, None]), 0.0)
    outer = outer.transpose(3, 0, 2, 1, 4).reshape(heads, 4, total_rows)
    peak = jnp.broadcast_to(peak.transpose(2, 0, 1).reshape(heads, 4, 1), (heads, 4, 128))
    inner = (in_gate - run).transpose(2, 0, 1, 3).reshape(heads, 4, length)
    column = run.transpose(2, 3, 0, 1).reshape(heads, length, 4)
    ratio = width_a // width_k

    def columns(rows, width, first):
        return pl.BlockSpec((rows, width), lambda h: (0, first + h))

    def by_head(*shape):
        return pl.BlockSpec((1,) + shape, lambda h: (h, 0, 0))

    return pl.pallas_call(
        mixer_kernel,
        grid=(heads,),
        in_specs=[
            columns(length, width_k, 0),
            columns(length, width_k, 0),
            columns(length, width_a, 0),
            columns(length, width_k, 0),
            columns(length, width_k, 0),
            columns(length, width_b, 0),
            columns(total_rows, width_k, ratio * heads),
            columns(total_rows, width_a, 0),
            columns(total_rows, width_k, (ratio + 1) * heads),
            columns(total_rows, width_b, (ratio + 2) * heads),
            by_head(4, length),
            by_head(4, total_rows),
            by_head(length, 4),
            by_head(4, 128),
            by_head(1, width_a),
            by_head(1, width_b),
        ],
        out_specs=[columns(length, width_a, 0), columns(length, width_b, 0)],
        out_shape=[
            jax.ShapeDtypeStruct((length, heads * width_a), jnp.bfloat16),
            jax.ShapeDtypeStruct((length, heads * width_b), jnp.bfloat16),
        ],
        cost_estimate=pl.CostEstimate(
            flops=4 * heads * length * total_rows * (2 * width_k + 2 * width_a),
            bytes_accessed=2 * packed.size * count,
            transcendentals=0,
        ),
    )(
        query_a, key_a, value_a, query_b, key_b, value_b,
        gathered, gathered, gathered, gathered,
        inner, outer, column, peak, gain_a[:, None, :], gain_b[:, None, :],
    )


def unit_kernel(q, k, v, every_k, every_v, inner, outer, column, peak, gain, share, heads):
    heads[0] = one_head(
        q[0], k[0], v[0], every_k[...].reshape(-1, every_k.shape[-1]),
        every_v[...].reshape(-1, every_v.shape[-1]),
        [inner[0, r : r + 1, :] for r in range(2)],
        [outer[0, r : r + 1, :] for r in range(2)],
        [column[0, :, r : r + 1] for r in range(2)],
        [peak[0, r : r + 1, 0:1] for r in range(2)],
        gain[...],
        share[0:1, 0:1],
    )


def mix_units(query_a, key_a, value_a, query_b, key_b, value_b, in_gate, forget_gate, gain_a, gain_b):
    heads = gain_a.shape[0]
    length = query_a.shape[0]
    width_k = query_a.shape[1] // heads
    width_a, width_b = gain_a.shape[1], gain_b.shape[1]
    count, mine = lax.axis_size("sp"), lax.axis_index("sp")

    def widen(array, axis):
        pads = [(0, 0)] * array.ndim
        pads[axis] = (0, width_a - width_b)
        return jnp.pad(array, pads)

    def cut(values, queries, keys, width):
        parts = []
        for h in range(heads):
            value = values[:, h * width : (h + 1) * width]
            parts.append(
                jnp.concatenate(
                    [
                        value if width == width_a else widen(value, 1),
                        queries[:, h * width_k : (h + 1) * width_k],
                        keys[:, h * width_k : (h + 1) * width_k],
                    ],
                    axis=1,
                )
            )
        return parts

    packed = jnp.stack(
        cut(value_a, query_a, key_a, width_a) + cut(value_b, query_b, key_b, width_b)
    )
    log_decay = jax.nn.log_sigmoid(forget_gate)
    gates = jnp.stack([in_gate, log_decay], axis=2)
    gates = gates.transpose(1, 3, 0, 2, 4).reshape(count, 4, length)
    gates = jnp.concatenate([gates, jnp.zeros_like(gates)], axis=1)
    rows, gates = exchange([packed, gates], 0)
    in_rows, decay = gates[:, 0:4:2], gates[:, 1:4:2]
    ones = jnp.ones((length, length), jnp.float32)
    exact = lax.Precision.HIGHEST
    run = jnp.stack(
        [
            jnp.dot(decay[:, 0], jnp.triu(ones), precision=exact),
            jnp.dot(decay[:, 1], jnp.tril(ones), precision=exact),
        ],
        axis=1,
    )
    whole = jnp.sum(decay, axis=-1)
    tails = in_rows + whole[..., None] - run
    place = jnp.arange(count)
    reader, source, middle = place[:, None, None], place[None, :, None], place[None, None, :]
    between = jnp.stack(
        [
            (middle > source) & (middle < reader),
            (middle < source) & (middle > reader),
        ],
        axis=1,
    ).astype(jnp.float32)
    gap = jnp.sum(between * whole.T[None, :, None, :], axis=-1)
    seen = jnp.stack([source < reader, source > reader], axis=1)
    logs = jnp.where(seen, tails.transpose(1, 0, 2)[None] + gap[..., None], NOTHING)
    peak = jnp.max(logs, axis=(2, 3))
    outer = jnp.where(seen, jnp.exp(logs - peak[:, :, None, None]), 0.0)
    outer = outer.reshape(count, 2, count * length)
    peak = jnp.broadcast_to(peak[:, :, None], (count, 2, 128))
    inner = in_rows - run
    column = run.transpose(0, 2, 1)
    gains = jnp.concatenate([gain_a, widen(gain_b, 1)], axis=0)
    gain = lax.dynamic_slice_in_dim(gains, mine, 1, 0)
    share = jnp.full((1, 128), jnp.where(mine < heads, 1.0 / width_a, 1.0 / width_b), jnp.float32)
    first_q, first_k = width_a // width_k, width_a // width_k + 1

    def block(width, first):
        return pl.BlockSpec((1, length, width), lambda t: (t, 0, first))

    def every(width, first):
        return pl.BlockSpec((count, length, width), lambda t: (0, 0, first))

    def by_block(*shape):
        return pl.BlockSpec((1,) + shape, lambda t: (t, 0, 0))

    def fixed(*shape):
        return pl.BlockSpec(shape, lambda t: (0, 0))

    out = pl.pallas_call(
        unit_kernel,
        grid=(count,),
        in_specs=[
            block(width_k, first_q),
            block(width_k, first_k),
            block(width_a, 0),
            every(width_k, first_k),
            every(width_a, 0),
            by_block(2, length),
            by_block(2, count * length),
            by_block(length, 2),
            by_block(2, 128),
            fixed(1, width_a),
            fixed(1, 128),
        ],
        out_specs=block(width_a, 0),
        out_shape=jax.ShapeDtypeStruct((count, length, width_a), jnp.bfloat16),
    )(rows, rows, rows, rows, rows, inner, outer, column, peak, gain, share)
    (units,) = exchange([out], 1)

    def lay(parts):
        return jnp.concatenate(parts, axis=1)

    return (
        lay([units[h] for h in range(heads)]),
        lay([units[heads + h][:, :width_b] for h in range(heads)]),
    )


def local(
    query_a,
    key_a,
    value_a,
    query_b,
    key_b,
    value_b,
    in_gate,
    forget_gate,
    head_gain_a,
    head_gain_b,
    out_weight_a,
    out_weight_b,
    residual,
    norm_gain,
    routes,
    route_weights,
    expert_gate,
    expert_up,
    expert_down,
):
    whole_heads = 2 * head_gain_a.shape[0] == lax.axis_size("sp")
    heads_a, heads_b = (mix_units if whole_heads else mix_heads)(
        query_a, key_a, value_a, query_b, key_b, value_b,
        in_gate, forget_gate, head_gain_a, head_gain_b,
    )
    first_term = jnp.einsum("ec,se->cs", out_weight_a, heads_a, preferred_element_type=jnp.float32)
    mix = lax.psum_scatter(
        (
            first_term
            + jnp.einsum("ec,se->cs", out_weight_b, heads_b, preferred_element_type=jnp.float32)
        ).astype(jnp.bfloat16),
        "tp",
        scatter_dimension=0,
        tiled=True,
    ).astype(jnp.float32)
    updated = residual.astype(jnp.float32) + mix
    squares = lax.psum(jnp.sum(updated * updated, axis=0), "tp")
    whole_width = residual.shape[0] * lax.axis_size("tp")
    normed = (
        updated * lax.rsqrt(squares / whole_width + EPSILON)[None, :] * norm_gain[:, None]
    ).astype(jnp.bfloat16)
    token_count = routes.shape[0]
    top_count = routes.shape[1]
    expert_count = lax.axis_size("sp") * expert_gate.shape[0]
    slot_count = 2 * token_count * top_count // expert_count
    flat_routes = routes.reshape(-1)
    hits = (flat_routes[:, None] == jnp.arange(expert_count, dtype=jnp.int32)[None, :]).astype(
        jnp.int32
    )
    ranks = jnp.sum((jnp.cumsum(hits, axis=0) - 1) * hits, axis=1)
    targets = (flat_routes * slot_count + ranks).reshape(token_count, top_count)
    slot_ids = jnp.arange(expert_count * slot_count, dtype=jnp.int32)[:, None]
    selectors = [
        (slot_ids == targets[None, :, ordering_index]).astype(jnp.bfloat16)
        for ordering_index in range(top_count)
    ]
    dispatch = selectors[0]
    ordering_index = 1
    dispatch = dispatch + selectors[ordering_index]
    buffer = jnp.einsum("ps,ds->pd", dispatch, normed, preferred_element_type=jnp.float32)
    buffer = buffer.astype(jnp.bfloat16).reshape(expert_count, slot_count, -1)
    piece = dispatch_rows(buffer, 2)
    flat_rows = piece.reshape(-1, piece.shape[-1])
    gate_rows = expert_gate[0]
    up_rows = expert_up[0]
    gate = jnp.dot(flat_rows, gate_rows, preferred_element_type=jnp.float32)
    upward = jnp.dot(flat_rows, up_rows, preferred_element_type=jnp.float32)
    hidden = (
        (jax.nn.silu(gate) * upward)
        .astype(jnp.bfloat16)
        .reshape(expert_count, slot_count, -1)
    )
    sources = hidden.shape[0]
    hidden_rows = hidden.reshape(-1, hidden.shape[-1])
    columns = expert_down[0]
    summed = lax.psum_scatter(
        jnp.einsum("rf,fc->cr", hidden_rows, columns, preferred_element_type=jnp.float32).astype(
            jnp.bfloat16
        ),
        "tp",
        scatter_dimension=0,
        tiled=True,
    ).astype(jnp.float32)
    outgoing = summed.astype(jnp.bfloat16).reshape(summed.shape[0], sources, slot_count)
    returned = lax.all_to_all(outgoing, "sp", split_axis=1, concat_axis=1, tiled=True)
    returned = returned.reshape(returned.shape[0], -1)
    combined = updated
    for ordering_index in range(top_count):
        picked = jnp.dot(returned, selectors[ordering_index], preferred_element_type=jnp.float32)
        combined = combined + route_weights[:, ordering_index][None, :] * picked
    return combined.astype(jnp.bfloat16)


def solution(mesh):
    placed = (
        P("sp", "tp"),
        P("sp", "tp"),
        P("sp", "tp"),
        P("sp", "tp"),
        P("sp", "tp"),
        P("sp", "tp"),
        P(None, None, "tp", "sp"),
        P(None, None, "tp", "sp"),
        P("tp", None),
        P("tp", None),
        P("tp", None),
        P("tp", None),
        P("tp", "sp"),
        P("tp"),
        P("sp", None),
        P("sp", None),
        P("sp", None, "tp"),
        P("sp", None, "tp"),
        P("sp", "tp", None),
    )
    return jax.shard_map(
        local, mesh=mesh, in_specs=placed, out_specs=P("tp", "sp"), check_vma=False
    )
```

profile of v0, /device:TPU:0, one launch (start us, length us, event | category | flops | bytes accessed | tf_op | source)
XLA Modules:
  0.0 219.8 jit_solution(2927015832219866738)
XLA Ops:
  6.5 1.1 fusion.90
  7.6 0.8 fusion.93
  8.5 0.9 slice_select_fusion
  9.3 0.7 fusion.77
  10.0 0.7 maximum_bitcast_fusion.5
  10.7 0.9 fusion.94
  11.7 0.9 fusion.91
  12.6 0.6 concatenate.44.refs_1_
  13.4 1.0 copy-done.1
  14.4 25.9 %shard_map.181 = (bf16[8,128,512]{2,1,0:T(8,128)(2,1)}, f32[8,8,128]{2,1,0:T(8,128)}) custom-call(bf16[8,128,512]{2,1,0:T(8,128)(2,1)} %copy-done.1, f32[8,8,128]{2,1,0:T(8,128)} %concatenate.44.refs_1_), custom_call_target="tpu_custom_call" | custom-call | tf_op jit(solution)/shard_map/pallas_call | solution.py:60
  40.3 0.8 slice.164
  41.1 0.8 slice.163
  41.9 0.1 convolution_bitcast_fusion
  42.1 0.2 convolution_bitcast_fusion.1
  42.3 1.1 copy.125
  43.4 0.6 fusion.88
  44.1 0.1 select_reduce_fusion.1
  44.3 0.2 select_reduce_fusion
  44.8 0.6 fusion.80.gain
  45.4 0.8 copy_select_fusion.1.outer
  46.2 0.7 broadcast_in_dim.63.peak
  46.8 0.5 broadcast_in_dim.64.share
  47.3 8.8 %shard_map.182.refs_0_ = bf16[8,128,256]{2,1,0:T(8,128)(2,1)} custom-call(bf16[8,128,512]{2,1,0:T(8,128)(2,1)} %get-tuple-element.7.q.k.v.every_k.every_v, bf16[8,128,512]{2,1,0:T(8,128)(2,1)} %get-tuple-element.7.q.k.v.every_k.every_v, bf16[8,128,512]{2,1,0:T(8,128)(2,1)} %get-tuple-element.7.q.k.v.every_k.every_v, ...), custom_call_target="tpu_custom_call" | custom-call | tf_op jit(solution)/shard_map/pallas_call | solution.py:404
  56.1 20.4 %shard_map.183 = bf16[8,128,256]{2,1,0:T(8,128)(2,1)} custom-call(bf16[8,128,256]{2,1,0:T(8,128)(2,1)} %shard_map.182.refs_0_), custom_call_target="tpu_custom_call" | custom-call | tf_op jit(solution)/shard_map/pallas_call | solution.py:60
  76.5 1.1 slice_bitcast_fusion.3
  77.6 2.9 %fusion.24 = f32[128,2048]{1,0:T(8,128)S(1)} fusion(bf16[1024,2048]{1,0:T(8,128)(2,1)} %param.29, bf16[128,256]{1,0:T(8,128)(2,1)S(1)} %get-tuple-element.13, bf16[128,256]{1,0:T(8,128)(2,1)S(1)} %get-tuple-element.14, bf16[128,256]{1,0:T(8,128)(2,1)S(1)} %get-tuple-element.15, bf16[128,256]{1,0:T(8,128)(2,1)S(1)} %get-tuple-element.16), kind=kOutput, calls=%fused_computation.24 | convolution fusion | flops 537919488 | bytes 5505024 | tf_op jit(solution)/shard_map/ec,se->cs/dot_general | solution.py:460
  80.6 1.3 fusion.13
  82.0 0.1 copy.127
  82.1 0.1 eq.60
  82.2 0.1 eq.56
  82.4 0.1 copy.114
  82.5 0.6 reduce-window.6
  83.1 0.2 slice_reduce_fusion
  83.4 0.1 fusion.78
  83.5 0.1 reduce_sum.41
  83.7 23.0 %reduce-scatter.3.cloned.1.call-done = bf16[512,128]{0,1:T(8,128)(2,1)} async-done(((bf16[2048,128]{0,1:T(8,128)(2,1)}), bf16[512,128]{0,1:T(8,128)(2,1)}) %reduce-scatter.3.cloned.1.call-update) | async-done | bytes 131088 | tf_op jit(solution)/shard_map/reduce_scatter | solution.py:461
  106.7 1.0 multiply_reduce_fusion
  107.7 5.8 %psum.7 = f32[128]{0:T(128)S(1)} all-reduce(f32[128]{0:T(128)S(1)} %multiply_reduce_fusion), channel_id=1, replica_groups=mesh['sp'=8,'tp'=4] {'tp'}, use_global_device_ids=true, to_apply=%region_8.9 | all-reduce | flops 128 | bytes 1024 | tf_op jit(solution)/shard_map/psum | solution.py:471
  113.5 2.1 convolution_convert_fusion
  115.6 26.6 %shard_map.184 = bf16[8,64,2048]{2,1,0:T(8,128)(2,1)} custom-call(bf16[8,64,512]{2,1,0:T(8,128)(2,1)} %bitcast.128), custom_call_target="tpu_custom_call" | custom-call | tf_op jit(solution)/shard_map/pallas_call | solution.py:155
  142.1 6.5 %fusion.4 = f32[512,1024]{1,0:T(8,128)} fusion(bf16[512,2048]{1,0:T(8,128)(2,1)} %bitcast.126, bf16[1,2048,1024]{2,1,0:T(8,128)(2,1)} %param.35), kind=kOutput, calls=%fused_computation.4 | convolution fusion | flops 2147483648 | bytes 8388608 | tf_op jit(solution)/shard_map/dot_general | solution.py:500
  148.6 10.5 %fusion.9 = bf16[2048,512]{0,1:T(8,128)(2,1)} fusion(bf16[1,1024,2048]{2,1,0:T(8,128)(2,1)} %param.37, f32[512,1024]{1,0:T(8,128)} %fusion.4, bf16[512,2048]{1,0:T(8,128)(2,1)} %bitcast.127, bf16[1,2048,1024]{2,1,0:T(8,128)(2,1)} %param.36), kind=kOutput, calls=%fused_computation.7 | convolution fusion | flops 4299161600 | bytes 14680064 | tf_op jit(solution)/shard_map/rf,fc->cr/dot_general | solution.py:511
  159.2 32.6 %reduce-scatter.5.cloned.1.call-done = bf16[512,512]{0,1:T(8,128)(2,1)} async-done(((bf16[2048,512]{0,1:T(8,128)(2,1)}), bf16[512,512]{0,1:T(8,128)(2,1)}) %reduce-scatter.5.cloned.1.call-update) | async-done | bytes 524304 | tf_op jit(solution)/shard_map/reduce_scatter | solution.py:510
  191.8 5.5 %all-to-all-start = ((bf16[512,8,64]{0,2,1:T(8,128)(2,1)}), bf16[512,8,64]{0,2,1:T(8,128)(2,1)S(1)}, u32[]{:S(2)}, u32[]{:S(2)}) async-start(bf16[512,8,64]{0,2,1:T(8,128)(2,1)} %bitcast.130), calls=%async_computation.2 | async-start | bytes 1048576 | tf_op jit(solution)/shard_map/all_to_all | solution.py:519
  197.4 14.3 %all-to-all-done = bf16[512,8,64]{0,2,1:T(8,128)(2,1)S(1)} async-done(((bf16[512,8,64]{0,2,1:T(8,128)(2,1)}), bf16[512,8,64]{0,2,1:T(8,128)(2,1)S(1)}, u32[]{:S(2)}, u32[]{:S(2)}) %all-to-all-start) | async-done | bytes 524320 | tf_op jit(solution)/shard_map/all_to_all | solution.py:519
  211.7 0.3 fusion.17
  212.0 0.3 fusion.18
  212.2 0.8 copy.132
  (58 shorter events, 0.9 us)
Async XLA Ops:
  6.5 74.0 %copy-start = (bf16[512,2048]{1,0:T(8,128)(2,1)S(1)}, bf16[512,2048]{1,0:T(8,128)(2,1)}, u32[]{:S(2)}) copy-start(bf16[512,2048]{1,0:T(8,128)(2,1)} %param.30) | copy-start | bytes 6291460
  6.5 100.2 %reduce-scatter.3.cloned.1.call-start = ((), (), s32[]{:S(2)}) async-start(), calls=%async_computation.3 | async-start | bytes 655360 | tf_op jit(solution)/shard_map/reduce_scatter | solution.py:461
  13.2 31.6 %copy-start.5 = (f32[4,256]{1,0:T(4,128)S(1)}, f32[4,256]{1,0:T(4,128)}, u32[]{:S(2)}) copy-start(f32[4,256]{1,0:T(4,128)} %param.27) | copy-start | bytes 12292
  13.2 31.6 %copy-start.7 = (f32[4,128]{1,0:T(4,128)S(1)}, f32[4,128]{1,0:T(4,128)}, u32[]{:S(2)}) copy-start(f32[4,128]{1,0:T(4,128)} %param.28) | copy-start | bytes 6148
  13.4 1.0 copy-start.1
  80.6 1.4 copy-start.4
  80.6 1.8 copy-start.3
  80.6 32.9 %copy-start.6 = (f32[512]{0:T(512)S(1)}, f32[512]{0:T(512)}, u32[]{:S(2)}) copy-start(f32[512]{0:T(512)} %param.32) | copy-start | bytes 6148
  81.9 109.9 %reduce-scatter.5.cloned.1.call-start = ((), (), s32[]{:S(2)}) async-start(), calls=%async_computation.4 | async-start | bytes 2621440 | tf_op jit(solution)/shard_map/reduce_scatter | solution.py:510
  159.2 38.2 %copy-start.8 = (f32[128,2]{0,1:T(2,128)S(1)}, f32[128,2]{0,1:T(2,128)}, u32[]{:S(2)}) copy-start(f32[128,2]{0,1:T(2,128)} %param.34) | copy-start | bytes 3076
  159.2 52.5 %copy-start.2 = (bf16[512,128]{0,1:T(8,128)(2,1)S(1)}, bf16[512,128]{0,1:T(8,128)(2,1)}, u32[]{:S(2)}) copy-start(bf16[512,128]{0,1:T(8,128)(2,1)} %reduce-scatter.3.cloned.1.call-done) | copy-start | bytes 393220
  191.8 19.8 %all-to-all-start = ((bf16[512,8,64]{0,2,1:T(8,128)(2,1)}), bf16[512,8,64]{0,2,1:T(8,128)(2,1)S(1)}, u32[]{:S(2)}, u32[]{:S(2)}) async-start(bf16[512,8,64]{0,2,1:T(8,128)(2,1)} %bitcast.130), calls=%async_computation.2 | async-start | bytes 1048576 | tf_op jit(solution)/shard_map/all_to_all | solution.py:519
Sparse Core Ops, SparseCore 0:
  82.0 24.6 reduce-scatter.2
  159.3 32.4 reduce-scatter.4
where the time goes:
time: 221 us; the launch traced here: 220 us
  Pallas kernels  81.6 us (37%)
  waiting for transfers between devices  70 us (32%)
  matrix products  24.2 us (11%)
  between operations  13.8 us (6%)
  local copies, waits for them, and re-layouts  12.4 us (6%)
  other arithmetic  6.56 us (3%)
  blocking collectives  5.75 us (3%)
  starting transfers between devices  5.55 us (3%)
    pallas_call x2, Pallas kernels, exchange(): pl.pallas_call(functools.partial(exchange_kernel, count, len(arrays)), ou...  46.2 us
    reduce_scatter x1, waiting for transfers between devices, local(): lax.psum_scatter(jnp.einsum('rf,fc->cr', hidden_rows, columns, preferred_...  32.6 us
    pallas_call x1, Pallas kernels, dispatch_rows(): pl.pallas_call(functools.partial(dispatch_kernel, count, across), out_sha...  26.6 us
    reduce_scatter x1, waiting for transfers between devices, local(): lax.psum_scatter((first_term + jnp.einsum('ec,se->cs', out_weight_b, head...  23 us
    all_to_all x1, waiting for transfers between devices, local(): lax.all_to_all(outgoing, 'sp', split_axis=1, concat_axis=1, tiled=True)  14.3 us
    dot_general x1, matrix products, local(): jnp.einsum('rf,fc->cr', hidden_rows, columns, preferred_element_type=jnp....  10.5 us
    pallas_call x1, Pallas kernels, mix_units(): pl.pallas_call(unit_kernel, grid=(count,), in_specs=[block(width_k, first...  8.8 us
    dot_general x1, matrix products, local(): gate = jnp.dot(flat_rows, gate_rows, preferred_element_type=jnp.float32)  6.49 us
  transfers between devices with their start and end apart: 3, of which 3 were waited for; matrix products, arithmetic and copies ran while one was open for 1% of the time, Pallas kernels for 0%

commit v1 on v0

--- a/solution.py
+++ b/solution.py
@@ -71,99 +71,254 @@
     )(*arrays)
 
 
-def dispatch_kernel(count, across, given, taken, sent, landed, kept, y_sent, y_landed, c_sent, c_landed):
+def moe_kernel(
+    count, across, given, gate_hbm, up_hbm, down_hbm, out,
+    rows, gate_w, up_w, down_w, hidden, part, partner, chip, cross, total,
+    kept, weight, sent, landed, y_sent, y_landed, c_sent, c_landed,
+    t_sent, t_landed, r_sent, r_landed, s_sent, s_landed,
+):
     mine, slot = lax.axis_index("sp"), lax.axis_index("tp")
     chips = across // 2
-    width = given.shape[-1]
-    twin = slot + 1 - 2 * lax.rem(slot, 2)
+    slots, width = given.shape[1], given.shape[2]
+    units = gate_w.shape[1]
+    core = lax.rem(slot, 2)
+    row = lax.div(slot, 2)
+    twin = slot + 1 - 2 * core
     others = [lax.rem(slot + 2 * step, across) for step in range(1, chips)]
     behind = [lax.rem(slot + across - 2 * step, across) for step in range(1, chips)]
-    peers = [lax.rem(mine + step, count) for step in range(1, count)]
-    greet([{"sp": peer} for peer in peers] + [{"tp": other} for other in others] + [{"tp": twin}])
-
-    def place(source, owner):
-        return taken.at[source, :, pl.ds(pl.multiple_of(owner * width, width), width)]
-
-    def forward(source, owner, target, send, land):
+    weights = [
+        pltpu.make_async_copy(source, target, weight.at[i])
+        for i, (source, target) in enumerate(
+            ((gate_hbm, gate_w), (up_hbm, up_w), (down_hbm, down_w))
+        )
+    ]
+    for copy in weights:
+        copy.start()
+    targets = [lax.rem(mine + step, count) for step in range(count)]
+    sources = [lax.rem(mine + count - step, count) for step in range(count)]
+    greet(
+        [{"sp": target} for target in targets[1:]]
+        + [{"tp": other} for other in others]
+        + [{"tp": twin}]
+    )
+
+    def remote(source, target, send, land, device):
         copy = pltpu.make_async_remote_copy(
-            src_ref=place(source, owner),
-            dst_ref=place(source, owner),
-            send_sem=send,
-            recv_sem=land,
-            device_id={"tp": target},
-            device_id_type=MESH,
+            src_ref=source, dst_ref=target, send_sem=send, recv_sem=land,
+            device_id=device, device_id_type=MESH,
         )
         copy.start()
         return copy
 
-    own = pltpu.make_async_copy(given.at[mine], place(mine, slot), kept.at[0])
-    own.start()
-    first = []
-    for step, peer in enumerate(peers):
-        copy = pltpu.make_async_remote_copy(
-            src_ref=given.at[peer],
-            dst_ref=place(mine, slot),
-            send_sem=sent.at[step],
-            recv_sem=landed.at[step],
-            device_id={"sp": peer},
-            device_id_type=MESH,
+    def place(step, owner):
+        return rows.at[step, :, pl.ds(pl.multiple_of(owner * width, width), width)]
+
+    first = [pltpu.make_async_copy(given.at[mine], place(0, slot), kept.at[0])]
+    first[0].start()
+    for step in range(1, count):
+        first.append(
+            remote(
+                given.at[targets[step]], place(step, slot), sent.at[step], landed.at[step],
+                {"sp": targets[step]},
+            )
         )
-        copy.start()
-        first.append(copy)
-    sources = [lax.rem(mine + count - step, count) for step in range(count)]
-    along, last = [], []
+    along = {}
+    last = {}
+
+    def relay(step):
+        if step == 0:
+            first[0].wait()
+        else:
+            first[step].wait_recv()
+        along[step] = [
+            remote(
+                place(step, slot), place(step, slot),
+                y_sent.at[step, turn], y_landed.at[step, turn], {"tp": other},
+            )
+            for turn, other in enumerate(others)
+        ]
+        last[step] = [
+            remote(
+                place(step, slot), place(step, slot),
+                c_sent.at[step, 0], c_landed.at[step, 0], {"tp": twin},
+            )
+        ]
 
     def hand_over(step):
         for turn, owner in enumerate(behind):
             along[step][turn].wait_recv()
-            last.append(
-                forward(
-                    sources[step], owner, twin, c_sent.at[step, turn + 1], c_landed.at[step, turn + 1]
+            last[step].append(
+                remote(
+                    place(step, owner), place(step, owner),
+                    c_sent.at[step, turn + 1], c_landed.at[step, turn + 1], {"tp": twin},
                 )
             )
 
+    half = count // 2
+    tile = min(256, units)
+    batch = half * slots
+
+    def arrive(steps):
+        for step in steps:
+            for copy in last[step]:
+                copy.wait_recv()
+
+    def lift(h, turns):
+        x = rows[h * half : (h + 1) * half].reshape(batch, width * across)
+        for turn in turns:
+            columns = slice(turn * tile, (turn + 1) * tile)
+            gate = dot(x, gate_w[:, columns], ((1,), (0,)))
+            upward = dot(x, up_w[:, columns], ((1,), (0,)))
+            hidden[h * batch : (h + 1) * batch, columns] = (
+                jax.nn.silu(gate) * upward
+            ).astype(jnp.bfloat16)
+
+    def lower(h, owners):
+        x = hidden[h * batch : (h + 1) * batch, :]
+        for owner in owners:
+            y = dot(x, down_w[:, owner * width : (owner + 1) * width], ((1,), (0,)))
+            part[owner, h * half : (h + 1) * half] = y.astype(jnp.bfloat16).reshape(
+                half, slots, width
+            )
+
+    pieces = 2
+    span = half // pieces
+    over, crossed, back = {}, {}, {}
+
+    def group(h, piece):
+        return pl.ds(h * half + piece * span, span)
+
+    def pass_twin(h):
+        for piece in range(pieces):
+            for y in range(chips):
+                block = group(h, piece)
+                over[h, piece, y] = remote(
+                    part.at[2 * y + 1 - core, block], partner.at[y, block],
+                    t_sent.at[h * pieces + piece, y], t_landed.at[h * pieces + piece, y],
+                    {"tp": twin},
+                )
+
+    def join_twin(h, piece):
+        block = group(h, piece)
+        for y in range(chips):
+            over[h, piece, y].wait_recv()
+        for turn in range(chips - 1):
+            y = lax.rem(row + turn + 1, chips)
+            chip[turn, block] = (
+                part[2 * y + core, block].astype(jnp.float32)
+                + partner[y, block].astype(jnp.float32)
+            ).astype(jnp.bfloat16)
+            crossed[h, piece, turn] = remote(
+                chip.at[turn, block], cross.at[turn, block],
+                r_sent.at[h * pieces + piece, turn], r_landed.at[h * pieces + piece, turn],
+                {"tp": others[turn]},
+            )
+
+    def give_back(h, piece):
+        block = group(h, piece)
+        value = part[2 * row + core, block].astype(jnp.float32) + partner[row, block].astype(
+            jnp.float32
+        )
+        for turn in range(chips - 1):
+            crossed[h, piece, turn].wait_recv()
+            value = value + cross[turn, block].astype(jnp.float32)
+        total[block] = value.astype(jnp.bfloat16)
+        for step in range(h * half + piece * span, h * half + (piece + 1) * span):
+            if step == 0:
+                back[step] = pltpu.make_async_copy(total.at[0], out.at[mine], kept.at[1])
+                back[step].start()
+            else:
+                back[step] = remote(
+                    total.at[step], out.at[mine], s_sent.at[step], s_landed.at[step],
+                    {"sp": sources[step]},
+                )
+
+    turns = list(range(units // tile))
+    cut = half + 1
+    relay(0)
+    for step in range(1, cut):
+        relay(step)
+        hand_over(step - 1)
+    weights[0].wait()
+    weights[1].wait()
+    arrive(range(half))
+    rest = list(range(cut, count))
+    work = [functools.partial(lift, 0, [turn]) for turn in turns]
+    work.append(weights[2].wait)
+    work += [functools.partial(lower, 0, [owner]) for owner in range(across)]
+    work.append(functools.partial(pass_twin, 0))
+    share = -(-len(work) // (len(rest) + 1))
+    for at in range(len(rest) + 1):
+        for thunk in work[at * share : (at + 1) * share]:
+            thunk()
+        if at < len(rest):
+            relay(rest[at])
+            hand_over(rest[at] - 1)
+    hand_over(count - 1)
+    for piece in range(pieces):
+        join_twin(0, piece)
+    arrive(range(half, count))
+    lift(1, turns)
+    for piece in range(pieces):
+        give_back(0, piece)
+    lower(1, range(across))
+    pass_twin(1)
+    for piece in range(pieces):
+        join_twin(1, piece)
+    for piece in range(pieces):
+        give_back(1, piece)
     for step in range(count):
         if step == 0:
-            own.wait()
+            back[0].wait()
         else:
-            first[step - 1].wait_recv()
-        along.append(
-            [
-                forward(sources[step], slot, other, y_sent.at[step, turn], y_landed.at[step, turn])
-                for turn, other in enumerate(others)
-            ]
-        )
-        last.append(forward(sources[step], slot, twin, c_sent.at[step, 0], c_landed.at[step, 0]))
-        if step > 0:
-            hand_over(step - 1)
-    hand_over(count - 1)
-    for copy in first:
+            first[step].wait_send()
+            back[step].wait()
+        for copy in along[step]:
+            copy.wait_send()
+        for copy in last[step]:
+            copy.wait_send()
+    for copy in list(over.values()) + list(crossed.values()):
         copy.wait_send()
-    for copies in along:
-        for copy in copies:
-            copy.wait_send()
-    for copy in last:
-        copy.wait()
-
-
-def dispatch_rows(buffer, number):
-    count, rows, width = buffer.shape
+
+
+def moe(given, gate, up, down, number):
+    count, slots, width = given.shape
     across = lax.axis_size("tp")
     chips = across // 2
-    spec = pl.BlockSpec(memory_space=pltpu.VMEM)
+    units = gate.shape[1]
+    vmem = pl.BlockSpec(memory_space=pltpu.VMEM)
+    whole = pl.BlockSpec(memory_space=pl.ANY)
     dma = pltpu.SemaphoreType.DMA
+    bf16 = jnp.bfloat16
+    pieces = 4
     return pl.pallas_call(
-        functools.partial(dispatch_kernel, count, across),
-        out_shape=jax.ShapeDtypeStruct((count, rows, width * across), buffer.dtype),
-        in_specs=[spec],
-        out_specs=spec,
+        functools.partial(moe_kernel, count, across),
+        out_shape=jax.ShapeDtypeStruct((count, slots, width), bf16),
+        in_specs=[vmem, whole, whole, whole],
+        out_specs=vmem,
         scratch_shapes=[
-            dma((count - 1,)), dma((count - 1,)), dma((1,)),
+            pltpu.VMEM((count, slots, width * across), bf16),
+            pltpu.VMEM(gate.shape, bf16),
+            pltpu.VMEM(up.shape, bf16),
+            pltpu.VMEM(down.shape, bf16),
+            pltpu.VMEM((count * slots, units), bf16),
+            pltpu.VMEM((across, count, slots, width), bf16),
+            pltpu.VMEM((chips, count, slots, width), bf16),
+            pltpu.VMEM((chips - 1, count, slots, width), bf16),
+            pltpu.VMEM((chips - 1, count, slots, width), bf16),
+            pltpu.VMEM((count, slots, width), bf16),
+            dma((2,)), dma((3,)),
+            dma((count,)), dma((count,)),
             dma((count, chips - 1)), dma((count, chips - 1)),
             dma((count, chips)), dma((count, chips)),
+            dma((pieces, chips)), dma((pieces, chips)),
+            dma((pieces, chips - 1)), dma((pieces, chips - 1)),
+            dma((count,)), dma((count,)),
         ],
-        compiler_params=pltpu.CompilerParams(collective_id=number, has_side_effects=True),
-    )(buffer)
+        compiler_params=pltpu.CompilerParams(
+            collective_id=number, has_side_effects=True, vmem_limit_bytes=48 * 1024 * 1024
+        ),
+    )(given, gate, up, down)
 
 
 def one_head(query, key, value, keys, values, inner_row, outer_row, column, peak, gain, share):
@@ -493,34 +648,13 @@
     dispatch = dispatch + selectors[ordering_index]
     buffer = jnp.einsum("ps,ds->pd", dispatch, normed, preferred_element_type=jnp.float32)
     buffer = buffer.astype(jnp.bfloat16).reshape(expert_count, slot_count, -1)
-    piece = dispatch_rows(buffer, 2)
-    flat_rows = piece.reshape(-1, piece.shape[-1])
-    gate_rows = expert_gate[0]
-    up_rows = expert_up[0]
-    gate = jnp.dot(flat_rows, gate_rows, preferred_element_type=jnp.float32)
-    upward = jnp.dot(flat_rows, up_rows, preferred_element_type=jnp.float32)
-    hidden = (
-        (jax.nn.silu(gate) * upward)
-        .astype(jnp.bfloat16)
-        .reshape(expert_count, slot_count, -1)
-    )
-    sources = hidden.shape[0]
-    hidden_rows = hidden.reshape(-1, hidden.shape[-1])
-    columns = expert_down[0]
-    summed = lax.psum_scatter(
-        jnp.einsum("rf,fc->cr", hidden_rows, columns, preferred_element_type=jnp.float32).astype(
-            jnp.bfloat16
-        ),
-        "tp",
-        scatter_dimension=0,
-        tiled=True,
-    ).astype(jnp.float32)
-    outgoing = summed.astype(jnp.bfloat16).reshape(summed.shape[0], sources, slot_count)
-    returned = lax.all_to_all(outgoing, "sp", split_axis=1, concat_axis=1, tiled=True)
-    returned = returned.reshape(returned.shape[0], -1)
+    returned = moe(buffer, expert_gate[0], expert_up[0], expert_down[0], 2)
+    returned = returned.reshape(-1, returned.shape[-1])
     combined = updated
     for ordering_index in range(top_count):
-        picked = jnp.dot(returned, selectors[ordering_index], preferred_element_type=jnp.float32)
+        picked = jnp.einsum(
+            "pd,ps->ds", returned, selectors[ordering_index], preferred_element_type=jnp.float32
+        )
         combined = combined + route_weights[:, ordering_index][None, :] * picked
     return combined.astype(jnp.bfloat16)
 

time: 221 us -> 180 us (0.81)
  waiting for transfers between devices: 70 us -> 23 us
  Pallas kernels: 81.6 us -> 109 us
  matrix products: 24.2 us -> 6.48 us
  starting transfers between devices: 5.55 us -> 0.01 us
    reduce_scatter x1 -> x0, waiting for transfers between devices: 32.6 us -> none  [local(): lax.psum_scatter(jnp.einsum('rf,fc->cr', hidden_rows, columns, preferred_...]
    pallas_call x1, Pallas kernels: 26.6 us -> 53.8 us  [moe(): pl.pallas_call(functools.partial(moe_kernel, count, across), out_shape=ja...]
    dot_general x4 -> x2, matrix products: 17.6 us -> 0.56 us  [local(): jnp.einsum('pd,ps->ds', returned, selectors[ordering_index], preferred_el...]
    all_to_all x1 -> x0, waiting for transfers between devices: 14.3 us -> none  [local(): lax.all_to_all(outgoing, 'sp', split_axis=1, concat_axis=1, tiled=True)]
    all_to_all x1 -> x0, starting transfers between devices: 5.5 us -> none  [local(): lax.all_to_all(outgoing, 'sp', split_axis=1, concat_axis=1, tiled=True)]
  transfers between devices with their start and end apart: 3 -> 1, of which waited for: 3 -> 1; matrix products, arithmetic and copies ran while one was open for 1% -> 1% of each run, Pallas kernels for 0% -> 0%
where the time goes in v1:
time: 180 us; the launch traced here: 179 us
  Pallas kernels  109 us (61%)
  waiting for transfers between devices  23 us (13%)
  local copies, waits for them, and re-layouts  14.6 us (8%)
  between operations  13.8 us (8%)
  other arithmetic  6.56 us (4%)
  matrix products  6.48 us (4%)
  blocking collectives  5.94 us (3%)
    pallas_call x1, Pallas kernels, moe(): pl.pallas_call(functools.partial(moe_kernel, count, across), out_shape=ja...  53.8 us
    pallas_call x2, Pallas kernels, exchange(): pl.pallas_call(functools.partial(exchange_kernel, count, len(arrays)), ou...  46.2 us
    reduce_scatter x1, waiting for transfers between devices, local(): lax.psum_scatter((first_term + jnp.einsum('ec,se->cs', out_weight_b, head...  23 us
    pallas_call x1, Pallas kernels, mix_units(): pl.pallas_call(unit_kernel, grid=(count,), in_specs=[block(width_k, first...  8.8 us
    psum x1, blocking collectives, local(): squares = lax.psum(jnp.sum(updated * updated, axis=0), 'tp')  5.94 us
  transfers between devices with their start and end apart: 1, of which 1 were waited for; matrix products, arithmetic and copies ran while one was open for 1% of the time, Pallas kernels for 0%

profile of v1, /device:TPU:0, one launch (start us, length us, event | category | flops | bytes accessed | tf_op | source)
XLA Modules:
  0.0 179.2 jit_solution(7349460843779981209)
XLA Ops:
  6.6 1.1 fusion.73
  7.7 0.8 fusion.76
  8.5 0.9 slice_select_fusion
  9.3 0.7 fusion.61
  10.0 0.7 maximum_bitcast_fusion.5
  10.8 0.9 fusion.77
  11.7 0.9 fusion.74
  12.6 0.6 concatenate.44.refs_1_
  13.4 1.0 copy-done.2
  14.4 25.9 %shard_map.181 = (bf16[8,128,512]{2,1,0:T(8,128)(2,1)}, f32[8,8,128]{2,1,0:T(8,128)}) custom-call(bf16[8,128,512]{2,1,0:T(8,128)(2,1)} %copy-done.2, f32[8,8,128]{2,1,0:T(8,128)} %concatenate.44.refs_1_), custom_call_target="tpu_custom_call" | custom-call | tf_op jit(solution)/shard_map/pallas_call | solution.py:60
  40.3 0.8 slice.164
  41.1 0.1 reduce_sum.38
  41.2 0.8 slice.163
  42.0 0.1 convolution_bitcast_fusion
  42.1 0.2 convolution_bitcast_fusion.1
  42.4 1.1 copy.125
  43.4 0.6 fusion.71
  44.0 0.1 copy.118
  44.1 0.1 select_reduce_fusion.1
  44.3 0.2 select_reduce_fusion
  44.5 0.1 copy.123
  44.7 0.1 broadcast_in_dim.58
  44.8 0.6 fusion.64.gain
  45.4 0.8 copy_select_fusion.1.outer
  46.2 0.7 broadcast_in_dim.63.peak
  46.9 0.5 broadcast_in_dim.64.share
  47.3 8.8 %shard_map.182.refs_0_ = bf16[8,128,256]{2,1,0:T(8,128)(2,1)} custom-call(bf16[8,128,512]{2,1,0:T(8,128)(2,1)} %get-tuple-element.7.q.k.v.every_k.every_v, bf16[8,128,512]{2,1,0:T(8,128)(2,1)} %get-tuple-element.7.q.k.v.every_k.every_v, bf16[8,128,512]{2,1,0:T(8,128)(2,1)} %get-tuple-element.7.q.k.v.every_k.every_v, ...), custom_call_target="tpu_custom_call" | custom-call | tf_op jit(solution)/shard_map/pallas_call | solution.py:559
  56.1 20.4 %shard_map.183 = bf16[8,128,256]{2,1,0:T(8,128)(2,1)} custom-call(bf16[8,128,256]{2,1,0:T(8,128)(2,1)} %shard_map.182.refs_0_), custom_call_target="tpu_custom_call" | custom-call | tf_op jit(solution)/shard_map/pallas_call | solution.py:60
  76.5 1.1 slice_bitcast_fusion.3
  77.7 3.0 %fusion.8 = f32[128,2048]{1,0:T(8,128)S(1)} fusion(bf16[1024,2048]{1,0:T(8,128)(2,1)} %param.29, bf16[128,256]{1,0:T(8,128)(2,1)S(1)} %get-tuple-element.13, bf16[128,256]{1,0:T(8,128)(2,1)S(1)} %get-tuple-element.14, bf16[128,256]{1,0:T(8,128)(2,1)S(1)} %get-tuple-element.15, bf16[128,256]{1,0:T(8,128)(2,1)S(1)} %get-tuple-element.16), kind=kOutput, calls=%fused_computation.15 | convolution fusion | flops 537919488 | bytes 5505024 | tf_op jit(solution)/shard_map/ec,se->cs/dot_general | solution.py:615
  80.7 1.3 fusion.1
  82.0 0.1 copy.127
  82.1 0.1 eq.60
  82.3 0.1 eq.56
  82.4 0.1 copy.114
  82.5 0.6 reduce-window.6
  83.1 0.2 slice_reduce_fusion
  83.4 0.1 fusion.62
  83.5 0.1 reduce_sum.41
  83.7 23.0 %reduce-scatter.2.cloned.1.call-done = bf16[512,128]{0,1:T(8,128)(2,1)} async-done(((bf16[2048,128]{0,1:T(8,128)(2,1)}), bf16[512,128]{0,1:T(8,128)(2,1)}) %reduce-scatter.2.cloned.1.call-update) | async-done | bytes 131088 | tf_op jit(solution)/shard_map/reduce_scatter | solution.py:616
  106.8 1.0 multiply_reduce_fusion
  107.8 5.9 %psum.7 = f32[128]{0:T(128)S(1)} all-reduce(f32[128]{0:T(128)S(1)} %multiply_reduce_fusion), channel_id=1, replica_groups=mesh['sp'=8,'tp'=4] {'tp'}, use_global_device_ids=true, to_apply=%region_8.9 | all-reduce | flops 128 | bytes 1024 | tf_op jit(solution)/shard_map/psum | solution.py:626
  113.8 1.3 convolution_convert_fusion
  115.0 2.2 %copy-done.1 = bf16[1,2048,1024]{2,1,0:T(8,128)(2,1)S(1)} copy-done((bf16[1,2048,1024]{2,1,0:T(8,128)(2,1)S(1)}, bf16[1,2048,1024]{2,1,0:T(8,128)(2,1)}, u32[]{:S(2)}) %copy-start.1) | copy-done | bytes 4194328
  117.2 53.8 %shard_map.184 = bf16[8,64,512]{2,1,0:T(8,128)(2,1)S(1)} custom-call(bf16[8,64,512]{2,1,0:T(8,128)(2,1)S(1)} %bitcast.107, bf16[2048,1024]{1,0:T(8,128)(2,1)S(1)} %bitcast.106, bf16[2048,1024]{1,0:T(8,128)(2,1)} %bitcast.108, bf16[1024,2048]{1,0:T(8,128)(2,1)} %bitcast.109), custom_call_target="tpu_custom_call" | custom-call | tf_op jit(solution)/shard_map/pallas_call | solution.py:294
  171.0 0.3 fusion.3
  171.3 0.3 fusion.4
  171.6 0.8 copy.132
  (53 shorter events, 0.5 us)
Async XLA Ops:
  6.5 74.2 %copy-start = (bf16[512,2048]{1,0:T(8,128)(2,1)S(1)}, bf16[512,2048]{1,0:T(8,128)(2,1)}, u32[]{:S(2)}) copy-start(bf16[512,2048]{1,0:T(8,128)(2,1)} %param.30) | copy-start | bytes 6291460
  6.5 38.3 %copy-start.6 = (f32[4,256]{1,0:T(4,128)S(1)}, f32[4,256]{1,0:T(4,128)}, u32[]{:S(2)}) copy-start(f32[4,256]{1,0:T(4,128)} %param.27) | copy-start | bytes 12292
  6.5 38.3 %copy-start.8 = (f32[4,128]{1,0:T(4,128)S(1)}, f32[4,128]{1,0:T(4,128)}, u32[]{:S(2)}) copy-start(f32[4,128]{1,0:T(4,128)} %param.28) | copy-start | bytes 6148
  6.5 100.2 %reduce-scatter.2.cloned.1.call-start = ((), (), s32[]{:S(2)}) async-start(), calls=%async_computation.1 | async-start | bytes 655360 | tf_op jit(solution)/shard_map/reduce_scatter | solution.py:616
  13.4 1.0 copy-start.2
  77.7 4.3 %copy-start.5 = (s32[128,2]{0,1:T(2,128)S(1)}, s32[128,2]{0,1:T(2,128)}, u32[]{:S(2)}) copy-start(s32[128,2]{0,1:T(2,128)} %param.33) | copy-start | bytes 3076
  77.7 4.7 %copy-start.4 = (bf16[512,128]{1,0:T(8,128)(2,1)S(1)}, bf16[512,128]{1,0:T(8,128)(2,1)}, u32[]{:S(2)}) copy-start(bf16[512,128]{1,0:T(8,128)(2,1)} %param.31) | copy-start | bytes 393220
  77.7 6.0 %copy-start.9 = (f32[128,2]{0,1:T(2,128)S(1)}, f32[128,2]{0,1:T(2,128)}, u32[]{:S(2)}) copy-start(f32[128,2]{0,1:T(2,128)} %param.34) | copy-start | bytes 3076
  77.7 36.1 %copy-start.7 = (f32[512]{0:T(512)S(1)}, f32[512]{0:T(512)}, u32[]{:S(2)}) copy-start(f32[512]{0:T(512)} %param.32) | copy-start | bytes 6148
  115.0 2.2 %copy-start.1 = (bf16[1,2048,1024]{2,1,0:T(8,128)(2,1)S(1)}, bf16[1,2048,1024]{2,1,0:T(8,128)(2,1)}, u32[]{:S(2)}) copy-start(bf16[1,2048,1024]{2,1,0:T(8,128)(2,1)} %param.35) | copy-start | bytes 12582916
  117.2 53.8 %copy-start.3 = (bf16[512,128]{0,1:T(8,128)(2,1)S(1)}, bf16[512,128]{0,1:T(8,128)(2,1)}, u32[]{:S(2)}) copy-start(bf16[512,128]{0,1:T(8,128)(2,1)} %reduce-scatter.2.cloned.1.call-done) | copy-start | bytes 393220
Sparse Core Ops, SparseCore 0:
  82.1 24.6 reduce-scatter.1

commit v2 on v0

v2 whole, which is shorter than its diff:
```python
import functools

import jax
import jax.numpy as jnp
from jax import lax
from jax.experimental import pallas as pl
from jax.experimental.pallas import tpu as pltpu
from jax.sharding import PartitionSpec as P

EPSILON = 1e-06
NOTHING = -1e30


def dot(left, right, contract):
    return lax.dot_general(
        left, right, (contract, ((), ())), preferred_element_type=jnp.float32
    )


MESH = pl.DeviceIdType.MESH


def greet(peers):
    barrier = pltpu.get_barrier_semaphore()
    for peer in peers:
        pl.semaphore_signal(barrier, inc=1, device_id=peer, device_id_type=MESH)
    pl.semaphore_wait(barrier, len(peers))


def one_head(query, key, value, keys, values, inner_row, outer_row, column, peak, gain, share):
    length, width_k = query.shape
    scale = width_k ** (-0.5)
    rows = lax.broadcasted_iota(jnp.int32, (length, length), 0)
    lanes = lax.broadcasted_iota(jnp.int32, (length, length), 1)
    near = dot(query, key, ((1,), (1,))) * scale
    far = dot(query, keys, ((1,), (1,))) * scale
    far_scores = [far * outer_row[r] for r in range(2)]
    far_sums = [jnp.sum(scores, axis=1, keepdims=True) for scores in far_scores]
    far_values = dot(
        jnp.concatenate([scores.astype(jnp.bfloat16) for scores in far_scores], axis=0),
        values,
        ((1,), (0,)),
    )
    both = None
    for r in range(2):
        keep = lanes <= rows if r == 0 else lanes >= rows
        logs = jnp.where(keep, column[r] + inner_row[r], NOTHING)
        carried_log = column[r] + peak[r]
        top = jnp.maximum(carried_log, jnp.max(logs, axis=1, keepdims=True))
        carried = jnp.exp(carried_log - top)
        scores = near * jnp.exp(logs - top)
        numer = carried * far_values[r * length : (r + 1) * length] + dot(
            scores.astype(jnp.bfloat16), value, ((1,), (0,))
        )
        denom = carried * far_sums[r] + jnp.sum(scores, axis=1, keepdims=True)
        out = numer / jnp.maximum(jnp.abs(denom), jnp.exp(-top))
        both = out if both is None else both + out
    mean = jnp.sum(both * both, axis=1, keepdims=True) * share
    return (both * lax.rsqrt(mean + EPSILON) * gain).astype(jnp.bfloat16)


def mixer_kernel(
    qa, ka, va, qb, kb, vb, all_ka, all_va, all_kb, all_vb,
    inner, outer, column, peak, gain_a, gain_b, heads_a, heads_b,
):
    parts = (
        (qa, ka, va, all_ka, all_va, gain_a, heads_a),
        (qb, kb, vb, all_kb, all_vb, gain_b, heads_b),
    )
    for g, (q, k, v, every_k, every_v, gain, heads) in enumerate(parts):
        heads[...] = one_head(
            q[...], k[...], v[...], every_k[...], every_v[...],
            [inner[0, 2 * r + g : 2 * r + g + 1, :] for r in range(2)],
            [outer[0, 2 * r + g : 2 * r + g + 1, :] for r in range(2)],
            [column[0, :, 2 * r + g : 2 * r + g + 1] for r in range(2)],
            [peak[0, 2 * r + g : 2 * r + g + 1, 0:1] for r in range(2)],
            gain[0],
            1.0 / gain.shape[-1],
        )


def mix_heads(query_a, key_a, value_a, query_b, key_b, value_b, in_gate, forget_gate, gain_a, gain_b):
    heads = gain_a.shape[0]
    length = query_a.shape[0]
    width_k = query_a.shape[1] // heads
    width_a, width_b = gain_a.shape[1], gain_b.shape[1]
    count, mine = lax.axis_size("sp"), lax.axis_index("sp")
    packed = jnp.concatenate([value_a, key_a, key_b, value_b], axis=1)
    gathered = lax.all_gather(packed, "sp", axis=0, tiled=True)
    total_rows = gathered.shape[0]
    log_decay = jax.nn.log_sigmoid(forget_gate)
    ones = jnp.ones((length, length), jnp.float32)
    exact = lax.Precision.HIGHEST
    run = jnp.stack(
        [
            jnp.einsum("ghs,st->ght", log_decay[0], jnp.triu(ones), precision=exact),
            jnp.einsum("ghs,st->ght", log_decay[1], jnp.tril(ones), precision=exact),
        ]
    )
    whole = jnp.sum(log_decay, axis=-1, keepdims=True)
    tails = in_gate + whole - run
    small = lax.all_gather(
        jnp.stack([tails, jnp.broadcast_to(whole, tails.shape)]), "sp", axis=0
    )
    every_tail, every_whole = small[:, 0], small[:, 1, ..., 0]
    place = jnp.arange(count)
    source, middle = place[:, None], place[None, :]
    between = jnp.stack(
        [
            (middle > source) & (middle < mine),
            (middle < source) & (middle > mine),
        ]
    ).astype(jnp.float32)
    gap = jnp.sum(between[:, :, :, None, None] * jnp.moveaxis(every_whole, 0, 1)[:, None], axis=2)
    seen = jnp.stack([place < mine, place > mine])[:, :, None, None, None]
    logs = jnp.where(seen, jnp.moveaxis(every_tail, 0, 1) + gap[..., None], NOTHING)
    peak = jnp.max(logs, axis=(1, 4))
    outer = jnp.where(seen, jnp.exp(logs - peak[:, None, :, :, None]), 0.0)
    outer = outer.transpose(3, 0, 2, 1, 4).reshape(heads, 4, total_rows)
    peak = jnp.broadcast_to(peak.transpose(2, 0, 1).reshape(heads, 4, 1), (heads, 4, 128))
    inner = (in_gate - run).transpose(2, 0, 1, 3).reshape(heads, 4, length)
    column = run.transpose(2, 3, 0, 1).reshape(heads, length, 4)
    ratio = width_a // width_k

    def columns(rows, width, first):
        return pl.BlockSpec((rows, width), lambda h: (0, first + h))

    def by_head(*shape):
        return pl.BlockSpec((1,) + shape, lambda h: (h, 0, 0))

    return pl.pallas_call(
        mixer_kernel,
        grid=(heads,),
        in_specs=[
            columns(length, width_k, 0),
            columns(length, width_k, 0),
            columns(length, width_a, 0),
            columns(length, width_k, 0),
            columns(length, width_k, 0),
            columns(length, width_b, 0),
            columns(total_rows, width_k, ratio * heads),
            columns(total_rows, width_a, 0),
            columns(total_rows, width_k, (ratio + 1) * heads),
            columns(total_rows, width_b, (ratio + 2) * heads),
            by_head(4, length),
            by_head(4, total_rows),
            by_head(length, 4),
            by_head(4, 128),
            by_head(1, width_a),
            by_head(1, width_b),
        ],
        out_specs=[columns(length, width_a, 0), columns(length, width_b, 0)],
        out_shape=[
            jax.ShapeDtypeStruct((length, heads * width_a), jnp.bfloat16),
            jax.ShapeDtypeStruct((length, heads * width_b), jnp.bfloat16),
        ],
        cost_estimate=pl.CostEstimate(
            flops=4 * heads * length * total_rows * (2 * width_k + 2 * width_a),
            bytes_accessed=2 * packed.size * count,
            transcendentals=0,
        ),
    )(
        query_a, key_a, value_a, query_b, key_b, value_b,
        gathered, gathered, gathered, gathered,
        inner, outer, column, peak, gain_a[:, None, :], gain_b[:, None, :],
    )


EXACT = lax.Precision.HIGHEST


def exact_dot(left, right, contract):
    return lax.dot_general(
        left, right, (contract, ((), ())), precision=EXACT, preferred_element_type=jnp.float32
    )


def flip(index, mask):
    bit, result = 1, index
    while bit <= mask:
        if mask & bit:
            result = result + bit * (1 - 2 * lax.rem(lax.div(index, bit), 2))
        bit = 2 * bit
    return result


def partners(mine, count):
    if count & (count - 1) == 0:
        peers = [flip(mine, step) for step in range(count)]
        return peers, peers
    ahead = [lax.rem(mine + step, count) for step in range(count)]
    return ahead, [lax.rem(mine + count - step, count) for step in range(count)]


def arrival_order(count):
    near, far = list(range(1, count // 2)), list(range(count // 2, count))
    order = [0]
    while near or far:
        if near:
            order.append(near.pop(0))
        if far:
            order.append(far.pop(0))
    return order


class Names:
    pass


def upright(row):
    length = row.shape[1]
    diagonal = lax.broadcasted_iota(jnp.int32, (length, length), 0) == lax.broadcasted_iota(
        jnp.int32, (length, length), 1
    )
    return jnp.sum(jnp.where(diagonal, row, jnp.zeros_like(row)), axis=1, keepdims=True)


def send(source, target, pair, at, device):
    copy = pltpu.make_async_remote_copy(
        src_ref=source, dst_ref=target, send_sem=pair[0].at[at], recv_sem=pair[1].at[at],
        device_id=device, device_id_type=MESH,
    )
    copy.start()
    return copy


def near_sums(near, far, v, values, outer, inner, column, peak, keep):
    far_scores = far * outer
    far_sum = jnp.sum(far_scores, axis=1, keepdims=True)
    far_values = dot(far_scores.astype(jnp.bfloat16), values, ((1,), (0,)))
    logs = jnp.where(keep, column + inner, NOTHING)
    far_log = column + peak
    top = jnp.maximum(far_log, jnp.max(logs, axis=1, keepdims=True))
    far_part = jnp.exp(far_log - top)
    scores = near * jnp.exp(logs - top)
    numer = far_part * far_values + dot(scores.astype(jnp.bfloat16), v, ((1,), (0,)))
    denom = far_part * far_sum + jnp.sum(scores, axis=1, keepdims=True)
    return numer, denom, top


def settle(numer, denom, top):
    return numer / jnp.maximum(jnp.abs(denom), jnp.exp(-top))


def gate_part(n):
    blocks = n.gates.shape[0]
    for r in range(2):
        for g in range(2):
            inputs, forget = n.in_gate[r, g], n.forget_gate[r, g]
            decay = jnp.minimum(forget, 0.0) - jnp.log1p(jnp.exp(-jnp.abs(forget)))
            at = 2 * r + g
            for h in range(blocks):
                n.gates[h, at : at + 1] = inputs[h : h + 1]
                n.gates[h, 4 + at : 5 + at] = decay[h : h + 1]


def mixer_part(n):
    blocks = n.gates.shape[0]
    mine = lax.axis_index("sp")
    part = lax.div(mine, blocks)
    at = lax.rem(mine, blocks)
    length = n.qa.shape[0]
    fields = (
        (n.ka, n.all_ka), (n.va, n.all_va), (n.qa, n.all_qa),
        (n.kb, n.all_kb), (n.vb, n.all_vb), (n.qb, n.all_qb),
    )

    def columns(field, target, head):
        width = target.shape[-1]
        return field.at[:, pl.ds(pl.multiple_of(head * width, width), width)]

    kept = [pltpu.make_async_copy(n.gates.at[at], n.all_gates.at[at], n.m_kept.at[6])]
    for f, (field, target) in enumerate(fields):
        kept.append(pltpu.make_async_copy(columns(field, target, at), target.at[at], n.m_kept.at[f]))
    for copy in kept:
        copy.start()
    went = []
    to, of = partners(at, blocks)
    peers, givers = to[1:], of[1:]
    for step, peer in enumerate(peers):
        went.append(
            send(
                n.gates.at[peer], n.all_gates.at[at], (n.m_sent, n.m_landed), (step, 6),
                {"sp": part * blocks + peer},
            )
        )
    for f, (field, target) in enumerate(fields):
        for step, peer in enumerate(peers):
            went.append(
                send(
                    columns(field, target, peer), target.at[at],
                    (n.m_sent, n.m_landed), (step, f), {"sp": part * blocks + peer},
                )
            )
    near = blocks - 1
    for copy in kept:
        copy.wait()
    for copy in went[:near]:
        copy.wait_recv()
    rows = lax.broadcasted_iota(jnp.int32, (length, length), 0)
    lanes = lax.broadcasted_iota(jnp.int32, (length, length), 1)
    upper = (rows <= lanes).astype(jnp.float32)
    lower = (rows >= lanes).astype(jnp.float32)
    ahead = lax.broadcasted_iota(jnp.int32, (4, 1), 0) < 2
    ahead_lane = lax.broadcasted_iota(jnp.int32, (length, 4), 1) < 2
    tails, wholes = [], []
    for b in range(blocks):
        inputs, decay = n.all_gates[b, 0:4], n.all_gates[b, 4:8]
        run = jnp.where(
            ahead,
            exact_dot(decay, upper, ((1,), (0,))),
            exact_dot(decay, lower, ((1,), (0,))),
        )
        n.column[b] = jnp.where(
            ahead_lane,
            exact_dot(lower, decay, ((1,), (1,))),
            exact_dot(upper, decay, ((1,), (1,))),
        )
        whole = jnp.sum(decay, axis=1, keepdims=True)
        n.inner[b] = inputs - run
        tails.append(inputs + whole - run)
        wholes.append(whole)
    nothing = jnp.zeros((4, 1), jnp.float32)
    before, after = [nothing], [nothing]
    for b in range(blocks - 1):
        before.append(before[-1] + wholes[b])
        after.insert(0, after[0] + wholes[blocks - 1 - b])
    ends = [tails[b] + jnp.where(ahead, after[b], before[b]) for b in range(blocks)]
    peak = functools.reduce(
        jnp.maximum, [jnp.max(logs, axis=1, keepdims=True) for logs in ends]
    )
    first = part == 0
    weights = [jnp.exp(logs - peak) for logs in ends]
    weights = [jnp.where(first, w[0:2], w[2:4]) for w in weights]
    n.note[2:4] = jnp.broadcast_to(jnp.where(first, peak[0:2], peak[2:4]), (2, length))
    for t in range(blocks):
        seen = []
        for b in range(blocks):
            if b < t:
                logs = tails[b] + sum(wholes[b + 1 : t], nothing)
                seen.append(jnp.where(ahead, logs, NOTHING))
            elif b > t:
                logs = tails[b] + sum(wholes[t + 1 : b], nothing)
                seen.append(jnp.where(ahead, NOTHING, logs))
            else:
                seen.append(jnp.full((4, length), NOTHING, jnp.float32))
        top = functools.reduce(
            jnp.maximum, [jnp.max(logs, axis=1, keepdims=True) for logs in seen]
        )
        for b in range(blocks):
            n.outer[t, :, b * length : (b + 1) * length] = jnp.where(
                seen[b] > 0.5 * NOTHING, jnp.exp(seen[b] - top), 0.0
            )
        n.peak[t] = jnp.broadcast_to(top, (4, length))
        n.offset[t] = jnp.broadcast_to(jnp.where(ahead, before[t], after[t]), (4, length))
    other = {"sp": lax.rem(mine + blocks, 2 * blocks)}
    n.note[4:8] = jnp.zeros((4, length), jnp.float32)
    states = []

    def landed(*waves):
        for wave in waves:
            for copy in went[(1 + wave) * near : (2 + wave) * near]:
                copy.wait_recv()

    def state(g):
        keys, values, memory, far = (
            (n.all_ka, n.all_va, n.memory_a, n.far_a), (n.all_kb, n.all_vb, n.memory_b, n.far_b)
        )[g]
        total, normal = None, None
        for b in range(blocks):
            key = keys[b].astype(jnp.float32).T * weights[b][g : g + 1]
            piece = dot(key.astype(jnp.bfloat16), values[b], ((1,), (0,)))
            total = piece if total is None else total + piece
            amount = exact_dot(weights[b], keys[b].astype(jnp.float32), ((1,), (0,)))[g : g + 1]
            normal = amount if normal is None else normal + amount
        memory[...] = total.astype(jnp.bfloat16)
        n.note[g : g + 1] = normal
        states.append(send(memory, far, (n.h_sent, n.h_landed), g, other))

    def local_pass(g, start, stop):
        q, k, v, shut, wide = (
            (n.all_qa, n.all_ka, n.all_va, n.shut_a, n.open_a),
            (n.all_qb, n.all_kb, n.all_vb, n.shut_b, n.open_b),
        )[g]
        scale = q.shape[-1] ** (-0.5)
        order = jnp.where(first, 1, -1)
        keeps = [(rows - lanes) * order >= 0, (lanes - rows) * order >= 0]

        @pl.loop(start, stop)
        def _(turn):
            t = lax.rem(at + 1 + turn, blocks)
            keys = k[...].reshape(blocks * length, k.shape[-1])
            values = v[...].reshape(blocks * length, v.shape[-1])
            near_scores = dot(q[t], k[t], ((1,), (1,))) * scale
            far_scores = dot(q[t], keys, ((1,), (1,))) * scale

            def pick(ref, i):
                ahead_row, behind_row = ref[t, g : g + 1], ref[t, 2 + g : 3 + g]
                if i == 0:
                    return jnp.where(first, ahead_row, behind_row)
                return jnp.where(first, behind_row, ahead_row)

            sums = []
            for i in range(2):
                forth, back = n.column[t, :, g : g + 1], n.column[t, :, 2 + g : 3 + g]
                column = jnp.where(first, forth, back) if i == 0 else jnp.where(first, back, forth)
                sums.append(
                    near_sums(
                        near_scores, far_scores, v[t], values, pick(n.outer, i),
                        pick(n.inner, i), column, pick(n.peak, i)[:, 0:1], keeps[i],
                    )
                )
            shut[t] = settle(*sums[0])
            wide[t] = sums[1][0]
            n.stat[t, :, 2 * g : 2 * g + 1] = sums[1][1]
            n.stat[t, :, 2 * g + 1 : 2 * g + 2] = sums[1][2]

    landed(0, 1)
    state(0)
    landed(2)
    local_pass(0, 0, blocks // 2)
    landed(3, 4)
    state(1)
    states.append(send(n.note, n.far_note, (n.h_sent, n.h_landed), 2, other))
    local_pass(0, blocks // 2, blocks)
    landed(5)
    local_pass(1, 0, blocks)
    for copy in states:
        copy.wait_recv()

    def give(t, g):
        source = (n.out_a, n.out_b)[g]
        target = (n.heads_a, n.heads_b)[g]
        width = source.shape[-1]
        return pltpu.make_async_remote_copy(
            src_ref=source.at[t],
            dst_ref=target.at[:, pl.ds(pl.multiple_of(at * width, width), width)],
            send_sem=n.o_sent.at[t, g],
            recv_sem=n.o_landed.at[at, g],
            device_id={"sp": part * blocks + t},
            device_id_type=MESH,
        )

    def keep(g):
        source = (n.out_a, n.out_b)[g]
        target = (n.heads_a, n.heads_b)[g]
        width = source.shape[-1]
        return pltpu.make_async_copy(
            source.at[at],
            target.at[:, pl.ds(pl.multiple_of(at * width, width), width)],
            n.m_kept.at[7 + g],
        )

    @pl.loop(0, blocks)
    def _(turn):
        t = lax.rem(at + 1 + turn, blocks)
        groups = (
            (n.all_qa, n.far_a, n.gain_a, n.shut_a, n.open_a, n.out_a),
            (n.all_qb, n.far_b, n.gain_b, n.shut_b, n.open_b, n.out_b),
        )
        for g, (q, far, gain, shut, wide, out) in enumerate(groups):
            scale = q.shape[-1] ** (-0.5)
            query = q[t]
            reach = dot(query, far[...], ((1,), (0,))) * scale
            reach_sum = (
                jnp.sum(query.astype(jnp.float32) * n.far_note[g : g + 1], axis=1, keepdims=True)
                * scale
            )
            column = jnp.where(first, n.column[t, :, 2 + g : 3 + g], n.column[t, :, g : g + 1])
            offset = jnp.where(
                first, n.offset[t, 2 + g : 3 + g, 0:1], n.offset[t, g : g + 1, 0:1]
            )
            log = column + offset + n.far_note[2 + g : 3 + g, 0:1]
            denom = n.stat[t, :, 2 * g : 2 * g + 1]
            old = n.stat[t, :, 2 * g + 1 : 2 * g + 2]
            top = jnp.maximum(old, log)
            kept_part, reach_part = jnp.exp(old - top), jnp.exp(log - top)
            both = shut[t] + settle(
                kept_part * wide[t] + reach_part * reach,
                kept_part * denom + reach_part * reach_sum,
                top,
            )
            mean = jnp.mean(both * both, axis=1, keepdims=True)
            out[t] = (
                both * lax.rsqrt(mean + EPSILON) * gain[pl.ds(at, 1), :]
            ).astype(jnp.bfloat16)

            @pl.when(t != at)
            def _():
                give(t, g).start()

    def finish():
        for copy in went:
            copy.wait_send()
        for copy in states:
            copy.wait_send()
        for peer in peers:
            for g in range(2):
                give(peer, g).wait_send()

    for g in range(2):
        keep(g).start()
    for g in range(2):
        keep(g).wait()
    for peer in givers:
        for g in range(2):
            width = (n.out_a, n.out_b)[g].shape[-1]
            pltpu.make_async_remote_copy(
                src_ref=(n.out_a, n.out_b)[g].at[at],
                dst_ref=(n.heads_a, n.heads_b)[g].at[
                    :, pl.ds(pl.multiple_of(peer * width, width), width)
                ],
                send_sem=n.o_sent.at[at, g],
                recv_sem=n.o_landed.at[peer, g],
                device_id={"sp": part * blocks + peer},
                device_id_type=MESH,
            ).wait_recv()
    return finish


def project_part(n, count, across):
    slot = lax.axis_index("tp")
    chips = across // 2
    core, row = lax.rem(slot, 2), lax.div(slot, 2)
    twin = slot + 1 - 2 * core
    width = n.residual.shape[0]
    tokens = n.residual.shape[1]
    slots = n.given.shape[1]
    for copy in n.out_weights:
        copy.wait()

    def block(owner):
        columns = pl.ds(pl.multiple_of(owner * width, width), width)
        return dot(n.heads_a[...], n.wa[:, columns], ((1,), (0,))) + dot(
            n.heads_b[...], n.wb[:, columns], ((1,), (0,))
        )

    to_twin, over = [], []
    for turn in range(chips):
        y = lax.rem(row + turn + 1, chips)
        n.mix_out[turn] = block(2 * y + 1 - core).astype(jnp.bfloat16)
        to_twin.append(
            send(n.mix_out.at[turn], n.mix_in.at[turn], (n.p_sent, n.p_landed), turn, {"tp": twin})
        )
        n.mix_own[turn] = block(2 * y + core)
    for turn in range(chips - 1):
        to_twin[turn].wait_recv()
        n.mix_chip[turn] = (n.mix_own[turn] + n.mix_in[turn].astype(jnp.float32)).astype(
            jnp.bfloat16
        )
        other = lax.rem(slot + 2 * (turn + 1), across)
        over.append(
            send(n.mix_chip.at[turn], n.mix_far.at[turn], (n.q_sent, n.q_landed), turn, {"tp": other})
        )
    experts = lax.broadcasted_iota(jnp.int32, (tokens, 128), 1)
    named = [upright(n.routes[k : k + 1, :]) for k in range(n.routes.shape[0])]
    hits = functools.reduce(jnp.logical_or, [experts == e for e in named])
    earlier = lax.broadcasted_iota(jnp.int32, (tokens, tokens), 0) > lax.broadcasted_iota(
        jnp.int32, (tokens, tokens), 1
    )
    ranks = dot(
        earlier.astype(jnp.float32).astype(jnp.bfloat16),
        hits.astype(jnp.float32).astype(jnp.bfloat16),
        ((1,), (0,)),
    )
    places = lax.broadcasted_iota(jnp.int32, (tokens, count * slots), 1).astype(jnp.float32)
    for k, e in enumerate(named):
        target = jnp.sum(
            jnp.where(experts == e, ranks, 0.0), axis=1, keepdims=True
        ) + e.astype(jnp.float32) * slots
        n.choice[k] = (places == target).astype(jnp.float32).astype(jnp.bfloat16)
    picks = functools.reduce(
        jnp.add, [n.choice[k].astype(jnp.float32) for k in range(len(named))]
    )
    picks = picks.T.astype(jnp.bfloat16)
    base = n.residual[...].astype(jnp.float32).T
    to_twin[chips - 1].wait_recv()
    base = base + (n.mix_own[chips - 1] + n.mix_in[chips - 1].astype(jnp.float32))
    for turn in range(chips - 1):
        over[turn].wait_recv()
        base = base + n.mix_far[turn].astype(jnp.float32)
    n.updated[...] = base
    n.squares[0] = exact_dot(jnp.ones((8, width), jnp.float32), base * base, ((1,), (1,)))
    told = []
    for step in range(1, across):
        told.append(
            send(
                n.squares.at[0], n.squares.at[step], (n.v_sent, n.v_landed), step - 1,
                {"tp": lax.rem(slot + step, across)},
            )
        )
    for copy in told:
        copy.wait_recv()
    squares = n.squares[0]
    for step in range(1, across):
        squares = squares + n.squares[step]
    factor = lax.rsqrt(squares[0:1] / (width * across) + EPSILON)
    factor = upright(factor)
    normed = (n.updated[...] * factor * n.norm_gain[...]).astype(jnp.bfloat16)
    n.given[...] = (
        dot(picks, normed, ((1,), (0,))).astype(jnp.bfloat16).reshape(count, slots, width)
    )

    def finish():
        for copy in to_twin + over + told:
            copy.wait_send()

    return finish


def moe_part(n, count, across):
    mine, slot = lax.axis_index("sp"), lax.axis_index("tp")
    chips = across // 2
    given, rows, hidden, part = n.given, n.rows, n.hidden, n.part
    partner, chip, cross, total, out = n.partner, n.chip, n.cross, n.total, n.returned
    slots, width = given.shape[1], given.shape[2]
    units = n.gate_w.shape[1]
    core = lax.rem(slot, 2)
    row = lax.div(slot, 2)
    twin = slot + 1 - 2 * core
    others = [lax.rem(slot + 2 * step, across) for step in range(1, chips)]
    behind = [lax.rem(slot + across - 2 * step, across) for step in range(1, chips)]
    targets, sources = partners(mine, count)
    order = arrival_order(count)

    def place(step, owner):
        return rows.at[step, :, pl.ds(pl.multiple_of(owner * width, width), width)]

    first = [pltpu.make_async_copy(given.at[mine], place(0, slot), n.kept.at[0])]
    first[0].start()
    first += [None] * (count - 1)
    for step in order[1:]:
        first[step] = send(
            given.at[targets[step]], place(order.index(step), slot), (n.sent, n.landed), step,
            {"sp": targets[step]},
        )
    along, last = {}, {}

    def relay(i):
        if i == 0:
            first[0].wait()
        else:
            first[order[i]].wait_recv()
        along[i] = [
            send(place(i, slot), place(i, slot), (n.y_sent, n.y_landed), (i, turn), {"tp": other})
            for turn, other in enumerate(others)
        ]
        last[i] = [
            send(place(i, slot), place(i, slot), (n.c_sent, n.c_landed), (i, 0), {"tp": twin})
        ]

    def hand_over(i):
        for turn, owner in enumerate(behind):
            along[i][turn].wait_recv()
            last[i].append(
                send(
                    place(i, owner), place(i, owner), (n.c_sent, n.c_landed),
                    (i, turn + 1), {"tp": twin},
                )
            )

    groups = 4
    span = count // groups
    tile = min(256, units)
    batch = span * slots
    over, crossed, back = {}, {}, {}

    def block(h):
        return pl.ds(h * span, span)

    def arrive(h):
        for i in range(h * span, (h + 1) * span):
            for copy in last[i]:
                copy.wait_recv()

    def lift(h):
        x = rows[h * span : (h + 1) * span].reshape(batch, width * across)
        for turn in range(units // tile):
            columns = slice(turn * tile, (turn + 1) * tile)
            gate = dot(x, n.gate_w[:, columns], ((1,), (0,)))
            upward = dot(x, n.up_w[:, columns], ((1,), (0,)))
            hidden[h * batch : (h + 1) * batch, columns] = (
                jax.nn.silu(gate) * upward
            ).astype(jnp.bfloat16)

    def lower(h):
        x = hidden[h * batch : (h + 1) * batch, :]
        ys = [lax.rem(row + turn + 1, chips) for turn in range(chips)]
        for whose in (1 - core, core):
            for turn, y in enumerate(ys):
                owner = 2 * y + whose
                columns = pl.ds(pl.multiple_of(owner * width, width), width)
                value = dot(x, n.down_w[:, columns], ((1,), (0,)))
                side = 0 if whose is not core else 1
                part[side, turn, block(h)] = value.astype(jnp.bfloat16).reshape(
                    span, slots, width
                )
                if side == 0:
                    over[h, turn] = send(
                        part.at[0, turn, block(h)], partner.at[turn, block(h)],
                        (n.t_sent, n.t_landed), (h, turn), {"tp": twin},
                    )

    def joined(h, turn):
        over[h, turn].wait_recv()
        return part[1, turn, block(h)].astype(jnp.float32) + partner[turn, block(h)].astype(
            jnp.float32
        )

    def join_twin(h):
        for turn in range(chips - 1):
            chip[turn, block(h)] = joined(h, turn).astype(jnp.bfloat16)
            crossed[h, turn] = send(
                chip.at[turn, block(h)], cross.at[turn, block(h)], (n.r_sent, n.r_landed),
                (h, turn), {"tp": others[turn]},
            )

    def give_back(h):
        value = joined(h, chips - 1)
        for turn in range(chips - 1):
            crossed[h, turn].wait_recv()
            value = value + cross[turn, block(h)].astype(jnp.float32)
        total[block(h)] = value.astype(jnp.bfloat16)
        for i in range(h * span, (h + 1) * span):
            step = order[i]
            if step == 0:
                back[step] = pltpu.make_async_copy(total.at[i], out.at[mine], n.kept.at[1])
                back[step].start()
            else:
                back[step] = send(
                    total.at[i], out.at[mine], (n.s_sent, n.s_landed), step,
                    {"sp": sources[step]},
                )

    def weights_in(picked):
        for copy in picked:
            copy.wait()

    tasks = {
        2 * span: [
            functools.partial(weights_in, n.expert_weights[:2]),
            functools.partial(arrive, 0), functools.partial(lift, 0),
        ],
        2 * span + 1: [
            functools.partial(weights_in, n.expert_weights[2:]), functools.partial(lower, 0),
        ],
        3 * span: [
            functools.partial(arrive, 1), functools.partial(lift, 1),
            functools.partial(join_twin, 0), functools.partial(lower, 1),
        ],
    }
    relay(0)
    for i in range(1, count):
        for task in tasks.get(i, []):
            task()
        relay(i)
        hand_over(i - 1)
    hand_over(count - 1)
    arrive(2)
    lift(2)
    join_twin(1)
    lower(2)
    give_back(0)
    arrive(3)
    join_twin(2)
    lift(3)
    lower(3)
    give_back(1)
    join_twin(3)
    give_back(2)
    give_back(3)
    back[0].wait()
    for i in range(count):
        if i > 0:
            first[i].wait_send()
            back[i].wait()
        for copy in along[i] + last[i]:
            copy.wait_send()
    for copy in list(over.values()) + list(crossed.values()):
        copy.wait_send()


def layer_kernel(count, across, names, mixing, *refs):
    n = Names()
    for name, ref in zip(names, refs):
        setattr(n, name, ref)
    mine, slot = lax.axis_index("sp"), lax.axis_index("tp")
    n.out_weights = [
        pltpu.make_async_copy(source, target, n.weight.at[i])
        for i, (source, target) in enumerate(((n.out_wa, n.wa), (n.out_wb, n.wb)))
    ]
    n.expert_weights = [
        pltpu.make_async_copy(source, target, n.weight.at[2 + i])
        for i, (source, target) in enumerate(
            ((n.gate, n.gate_w), (n.up, n.up_w), (n.down, n.down_w))
        )
    ]
    peers = [{"sp": lax.rem(mine + step, count)} for step in range(1, count)]
    peers += [{"tp": lax.rem(slot + step, across)} for step in range(1, across)]
    barrier = pltpu.get_barrier_semaphore()
    for peer in peers:
        pl.semaphore_signal(barrier, inc=1, device_id=peer, device_id_type=MESH)
    for copy in n.out_weights + n.expert_weights:
        copy.start()
    if mixing:
        gate_part(n)
    pl.semaphore_wait(barrier, len(peers))
    done = []
    if mixing:
        done.append(mixer_part(n))
    done.append(project_part(n, count, across))
    moe_part(n, count, across)
    result = n.updated[...]
    returned = n.returned[...].reshape(-1, n.returned.shape[-1])
    for k in range(n.choice.shape[0]):
        result = result + upright(n.route_weights[k : k + 1, :]) * dot(
            n.choice[k], returned, ((1,), (0,))
        )
    n.out[...] = result.T.astype(jnp.bfloat16)
    for finish in done:
        finish()


def layer(mixer, others, weights, count, across, slots, number):
    bf16, f32 = jnp.bfloat16, jnp.float32
    vmem = pl.BlockSpec(memory_space=pltpu.VMEM)
    whole = pl.BlockSpec(memory_space=pl.ANY)
    dma = pltpu.SemaphoreType.DMA
    chips = across // 2
    width, tokens = others["residual"].shape
    top = others["routes"].shape[0]
    units = weights["gate"].shape[1]
    mixing = "qa" in mixer
    pieces = 4
    scratch = {}

    def buffer(name, shape, dtype=bf16):
        scratch[name] = pltpu.VMEM(shape, dtype)

    def pair(name, shape):
        scratch[name + "_sent"] = dma(shape)
        scratch[name + "_landed"] = dma(shape)

    if mixing:
        blocks = mixer["gain_a"].shape[0]
        wide_a, wide_b = mixer["gain_a"].shape[1], mixer["gain_b"].shape[1]
        dk = mixer["qa"].shape[1] // blocks
        for g, wide in (("a", wide_a), ("b", wide_b)):
            buffer("all_q" + g, (blocks, tokens, dk))
            buffer("all_k" + g, (blocks, tokens, dk))
            buffer("all_v" + g, (blocks, tokens, wide))
            buffer("memory_" + g, (dk, wide))
            buffer("far_" + g, (dk, wide))
            buffer("out_" + g, (blocks, tokens, wide))
            buffer("shut_" + g, (blocks, tokens, wide), f32)
            buffer("open_" + g, (blocks, tokens, wide), f32)
            buffer("heads_" + g, (tokens, blocks * wide))
        buffer("gates", (blocks, 8, tokens), f32)
        buffer("all_gates", (blocks, 8, tokens), f32)
        buffer("note", (8, tokens), f32)
        buffer("far_note", (8, tokens), f32)
        buffer("column", (blocks, tokens, 4), f32)
        buffer("stat", (blocks, tokens, 4), f32)
        buffer("inner", (blocks, 4, tokens), f32)
        buffer("outer", (blocks, 4, blocks * tokens), f32)
        buffer("peak", (blocks, 4, tokens), f32)
        buffer("offset", (blocks, 4, tokens), f32)
        scratch["m_kept"] = dma((9,))
        pair("m", (blocks - 1, 7))
        pair("h", (3,))
        pair("o", (blocks, 2))
    buffer("wa", weights["out_wa"].shape)
    buffer("wb", weights["out_wb"].shape)
    buffer("mix_out", (chips, tokens, width))
    buffer("mix_in", (chips, tokens, width))
    buffer("mix_own", (chips, tokens, width), f32)
    buffer("mix_chip", (chips - 1, tokens, width))
    buffer("mix_far", (chips - 1, tokens, width))
    buffer("updated", (tokens, width), f32)
    buffer("squares", (across, 8, tokens), f32)
    buffer("choice", (top, tokens, count * slots))
    buffer("given", (count, slots, width))
    buffer("returned", (count, slots, width))
    buffer("rows", (count, slots, width * across))
    buffer("gate_w", weights["gate"].shape)
    buffer("up_w", weights["up"].shape)
    buffer("down_w", weights["down"].shape)
    buffer("hidden", (count * slots, units))
    buffer("part", (2, chips, count, slots, width))
    buffer("partner", (chips, count, slots, width))
    buffer("chip", (chips - 1, count, slots, width))
    buffer("cross", (chips - 1, count, slots, width))
    buffer("total", (count, slots, width))
    scratch["kept"] = dma((2,))
    scratch["weight"] = dma((5,))
    pair("p", (chips,))
    pair("q", (chips - 1,))
    pair("v", (across - 1,))
    scratch["sent"], scratch["landed"] = dma((count,)), dma((count,))
    pair("y", (count, chips - 1))
    pair("c", (count, chips))
    pair("t", (pieces, chips))
    pair("r", (pieces, chips - 1))
    pair("s", (count,))
    inputs = {**mixer, **others, **weights}
    names = list(inputs) + ["out"] + list(scratch)
    return pl.pallas_call(
        functools.partial(layer_kernel, count, across, names, mixing),
        out_shape=jax.ShapeDtypeStruct((width, tokens), bf16),
        in_specs=[whole if name in weights else vmem for name in inputs],
        out_specs=vmem,
        scratch_shapes=list(scratch.values()),
        compiler_params=pltpu.CompilerParams(
            collective_id=number, has_side_effects=True, vmem_limit_bytes=56 * 1024 * 1024
        ),
    )(*inputs.values())


def local(
    query_a,
    key_a,
    value_a,
    query_b,
    key_b,
    value_b,
    in_gate,
    forget_gate,
    head_gain_a,
    head_gain_b,
    out_weight_a,
    out_weight_b,
    residual,
    norm_gain,
    routes,
    route_weights,
    expert_gate,
    expert_up,
    expert_down,
):
    count, across = lax.axis_size("sp"), lax.axis_size("tp")
    heads = head_gain_a.shape[0]
    if 2 * heads == count:
        mixer = dict(
            qa=query_a, ka=key_a, va=value_a, qb=query_b, kb=key_b, vb=value_b,
            in_gate=in_gate, forget_gate=forget_gate, gain_a=head_gain_a, gain_b=head_gain_b,
        )
    else:
        heads_a, heads_b = mix_heads(
            query_a, key_a, value_a, query_b, key_b, value_b,
            in_gate, forget_gate, head_gain_a, head_gain_b,
        )
        mixer = dict(heads_a=heads_a, heads_b=heads_b)
    token_count, top_count = routes.shape
    expert_count = count * expert_gate.shape[0]
    slots = 2 * token_count * top_count // expert_count
    others = dict(
        residual=residual, norm_gain=norm_gain[None, :], routes=routes.T,
        route_weights=route_weights.T,
    )
    weights = dict(
        out_wa=out_weight_a, out_wb=out_weight_b,
        gate=expert_gate[0], up=expert_up[0], down=expert_down[0],
    )
    return layer(mixer, others, weights, count, across, slots, 0)


def solution(mesh):
    placed = (
        P("sp", "tp"),
        P("sp", "tp"),
        P("sp", "tp"),
        P("sp", "tp"),
        P("sp", "tp"),
        P("sp", "tp"),
        P(None, None, "tp", "sp"),
        P(None, None, "tp", "sp"),
        P("tp", None),
        P("tp", None),
        P("tp", None),
        P("tp", None),
        P("tp", "sp"),
        P("tp"),
        P("sp", None),
        P("sp", None),
        P("sp", None, "tp"),
        P("sp", None, "tp"),
        P("sp", "tp", None),
    )
    return jax.shard_map(
        local, mesh=mesh, in_specs=placed, out_specs=P("tp", "sp"), check_vma=False
    )
```

time: 221 us -> 83.5 us (0.38)
  waiting for transfers between devices: 70 us -> 0 us
  matrix products: 24.2 us -> 0 us
  between operations: 13.8 us -> 0.01 us
  local copies, waits for them, and re-layouts: 12.4 us -> 1.57 us
  other arithmetic: 6.56 us -> 0 us
  blocking collectives: 5.75 us -> 0 us
  starting transfers between devices: 5.55 us -> 0 us
    reduce_scatter x2 -> x0, waiting for transfers between devices: 55.7 us -> none  [the longest x1 32.6 us: local(): lax.psum_scatter(jnp.einsum('rf,fc->cr', hidden_rows, columns, preferred_...]
    dot_general x9 -> x0, matrix products: 24.2 us -> none  [the longest x1 10.5 us: local(): jnp.einsum('rf,fc->cr', hidden_rows, columns, preferred_element_type=jnp....]
    all_to_all x1 -> x0, waiting for transfers between devices: 14.3 us -> none  [local(): lax.all_to_all(outgoing, 'sp', split_axis=1, concat_axis=1, tiled=True)]
    psum x1 -> x0, blocking collectives: 5.75 us -> none  [local(): squares = lax.psum(jnp.sum(updated * updated, axis=0), 'tp')]
    all_to_all x1 -> x0, starting transfers between devices: 5.5 us -> none  [local(): lax.all_to_all(outgoing, 'sp', split_axis=1, concat_axis=1, tiled=True)]
    slice x12 -> x0, local copies, waits for them, and re-layouts: 5.5 us -> none  [the longest x2 1.91 us: cut(): value = values[:, h * width:(h + 1) * width]]
    pallas_call x4 -> x1, Pallas kernels: 81.6 us -> 81.8 us  [layer(): pl.pallas_call(functools.partial(layer_kernel, count, across, names, mixi...]
  transfers between devices with their start and end apart: 3 -> 0, of which waited for: 3 -> 0; matrix products, arithmetic and copies ran while one was open for 1% -> 0% of each run, Pallas kernels for 0% -> 0%
where the time goes in v2:
time: 83.5 us; the launch traced here: 83.3 us
  Pallas kernels  81.8 us (98%)
  local copies, waits for them, and re-layouts  1.57 us (2%)
    pallas_call x1, Pallas kernels, layer(): pl.pallas_call(functools.partial(layer_kernel, count, across, names, mixi...  81.8 us

profile of v2, /device:TPU:0, one launch (start us, length us, event | category | flops | bytes accessed | tf_op | source)
XLA Modules:
  0.0 83.3 jit_solution(5738369850495302575)
XLA Ops:
  0.0 81.8 %shard_map.181 = bf16[512,128]{1,0:T(8,128)(2,1)} custom-call(bf16[128,512]{1,0:T(8,128)(2,1)} %refs_0_.1, bf16[128,512]{1,0:T(8,128)(2,1)} %refs_1_.1, bf16[128,1024]{1,0:T(8,128)(2,1)} %refs_2_.1, bf16[128,512]{1,0:T(8,128)(2,1)} %refs_3_.1, bf16[128,512]{1,0:T(8,128)(2,1)} %refs_4_.1, bf16[128,512]{1,0:T(8,128)(2,1)} %refs_5_.1, ...), custom_call_target="tpu_custom_call" | custom-call | tf_op jit(solution)/shard_map/pallas_call | solution.py:907
  81.8 1.6 %copy.21 = bf16[512,128]{1,0:T(8,128)(2,1)} copy(bf16[512,128]{1,0:T(8,128)(2,1)} %shard_map.181) | data formatting | bytes 262144

commit v3 on v2

--- a/solution.py
+++ b/solution.py
@@ -536,22 +536,26 @@
         )
 
     to_twin, over = [], []
+
+    def cross(turn):
+        to_twin[turn].wait_recv()
+        n.mix_chip[turn] = (n.mix_own[turn] + n.mix_in[turn].astype(jnp.float32)).astype(
+            jnp.bfloat16
+        )
+        other = lax.rem(slot + 2 * (turn + 1), across)
+        over.append(
+            send(n.mix_chip.at[turn], n.mix_far.at[turn], (n.q_sent, n.q_landed), turn, {"tp": other})
+        )
+
     for turn in range(chips):
         y = lax.rem(row + turn + 1, chips)
         n.mix_out[turn] = block(2 * y + 1 - core).astype(jnp.bfloat16)
         to_twin.append(
             send(n.mix_out.at[turn], n.mix_in.at[turn], (n.p_sent, n.p_landed), turn, {"tp": twin})
         )
+        if turn > 0:
+            cross(turn - 1)
         n.mix_own[turn] = block(2 * y + core)
-    for turn in range(chips - 1):
-        to_twin[turn].wait_recv()
-        n.mix_chip[turn] = (n.mix_own[turn] + n.mix_in[turn].astype(jnp.float32)).astype(
-            jnp.bfloat16
-        )
-        other = lax.rem(slot + 2 * (turn + 1), across)
-        over.append(
-            send(n.mix_chip.at[turn], n.mix_far.at[turn], (n.q_sent, n.q_landed), turn, {"tp": other})
-        )
     experts = lax.broadcasted_iota(jnp.int32, (tokens, 128), 1)
     named = [upright(n.routes[k : k + 1, :]) for k in range(n.routes.shape[0])]
     hits = functools.reduce(jnp.logical_or, [experts == e for e in named])
@@ -589,17 +593,27 @@
                 {"tp": lax.rem(slot + step, across)},
             )
         )
-    for copy in told:
-        copy.wait_recv()
-    squares = n.squares[0]
-    for step in range(1, across):
-        squares = squares + n.squares[step]
-    factor = lax.rsqrt(squares[0:1] / (width * across) + EPSILON)
-    factor = upright(factor)
-    normed = (n.updated[...] * factor * n.norm_gain[...]).astype(jnp.bfloat16)
+    raw = (n.updated[...] * n.norm_gain[...]).astype(jnp.bfloat16)
     n.given[...] = (
-        dot(picks, normed, ((1,), (0,))).astype(jnp.bfloat16).reshape(count, slots, width)
-    )
+        dot(picks, raw, ((1,), (0,))).astype(jnp.bfloat16).reshape(count, slots, width)
+    )
+
+    def spread():
+        for copy in told:
+            copy.wait_recv()
+        squares = n.squares[0]
+        for step in range(1, across):
+            squares = squares + n.squares[step]
+        factor = lax.rsqrt(squares / (width * across) + EPSILON)
+        chosen = functools.reduce(
+            jnp.add, [n.choice[k].astype(jnp.float32) for k in range(len(named))]
+        )
+        placed = exact_dot(factor, chosen, ((1,), (0,)))
+        n.factor[...] = jnp.zeros(n.factor.shape, jnp.float32)
+        for e in range(count):
+            n.factor[e, :, 0:slots] = placed[:, e * slots : (e + 1) * slots]
+
+    n.spread = spread
 
     def finish():
         for copy in to_twin + over + told:
@@ -623,6 +637,18 @@
     targets, sources = partners(mine, count)
     order = arrival_order(count)
 
+    scales = {}
+
+    def scale_out():
+        n.spread()
+        for i in range(1, count):
+            step = order[i]
+            scales[i] = send(
+                n.factor.at[targets[step]], n.factor_in.at[i], (n.f_sent, n.f_landed), i,
+                {"sp": targets[step]},
+            )
+        n.factor_in[0] = n.factor[mine]
+
     def place(step, owner):
         return rows.at[step, :, pl.ds(pl.multiple_of(owner * width, width), width)]
 
@@ -675,10 +701,16 @@
 
     def lift(h):
         x = rows[h * span : (h + 1) * span].reshape(batch, width * across)
+        factors = []
+        for i in range(h * span, (h + 1) * span):
+            if i > 0:
+                scales[i].wait_recv()
+            factors.append(upright(n.factor_in[i, 0:1])[0:slots])
+        factor = jnp.concatenate(factors, axis=0)
         for turn in range(units // tile):
             columns = slice(turn * tile, (turn + 1) * tile)
-            gate = dot(x, n.gate_w[:, columns], ((1,), (0,)))
-            upward = dot(x, n.up_w[:, columns], ((1,), (0,)))
+            gate = factor * dot(x, n.gate_w[:, columns], ((1,), (0,)))
+            upward = factor * dot(x, n.up_w[:, columns], ((1,), (0,)))
             hidden[h * batch : (h + 1) * batch, columns] = (
                 jax.nn.silu(gate) * upward
             ).astype(jnp.bfloat16)
@@ -750,6 +782,7 @@
         ],
     }
     relay(0)
+    scale_out()
     for i in range(1, count):
         for task in tasks.get(i, []):
             task()
@@ -774,6 +807,7 @@
         if i > 0:
             first[i].wait_send()
             back[i].wait()
+            scales[i].wait_send()
         for copy in along[i] + last[i]:
             copy.wait_send()
     for copy in list(over.values()) + list(crossed.values()):
@@ -878,6 +912,9 @@
     buffer("mix_far", (chips - 1, tokens, width))
     buffer("updated", (tokens, width), f32)
     buffer("squares", (across, 8, tokens), f32)
+    buffer("factor", (count, 8, 128), f32)
+    buffer("factor_in", (count, 8, 128), f32)
+    pair("f", (count,))
     buffer("choice", (top, tokens, count * slots))
     buffer("given", (count, slots, width))
     buffer("returned", (count, slots, width))

time: 83.5 us -> 82.8 us (level)
  no operation moved by 1% of the time
where the time goes in v3:
time: 82.8 us; the launch traced here: 82.6 us
  Pallas kernels  81.1 us (98%)
  local copies, waits for them, and re-layouts  1.57 us (2%)
    pallas_call x1, Pallas kernels, layer(): pl.pallas_call(functools.partial(layer_kernel, count, across, names, mixi...  81.1 us

profile of v3, /device:TPU:0, one launch (start us, length us, event | category | flops | bytes accessed | tf_op | source)
XLA Modules:
  0.0 82.6 jit_solution(13562334719980010954)
XLA Ops:
  0.0 81.1 %shard_map.181 = bf16[512,128]{1,0:T(8,128)(2,1)} custom-call(bf16[128,512]{1,0:T(8,128)(2,1)} %refs_0_.1, bf16[128,512]{1,0:T(8,128)(2,1)} %refs_1_.1, bf16[128,1024]{1,0:T(8,128)(2,1)} %refs_2_.1, bf16[128,512]{1,0:T(8,128)(2,1)} %refs_3_.1, bf16[128,512]{1,0:T(8,128)(2,1)} %refs_4_.1, bf16[128,512]{1,0:T(8,128)(2,1)} %refs_5_.1, ...), custom_call_target="tpu_custom_call" | custom-call | tf_op jit(solution)/shard_map/pallas_call | solution.py:944
  81.1 1.6 %copy.21 = bf16[512,128]{1,0:T(8,128)(2,1)} copy(bf16[512,128]{1,0:T(8,128)(2,1)} %shard_map.181) | data formatting | bytes 262144
